TPU v7x, 32 devices: a whole 2x2x4 slice. The times are simulated.
32 devices in a mesh: sp: 8 (over z, x), dp: 4 (over y, core).
Axes of the slice: x: 2, y: 2, z: 4, core: 2. Of those that a mesh axis runs over, the one named last changes fastest.
Arguments:
- queries: bfloat16 [4, 1024, 2048], P('dp', 'sp'), may hold values from -6 to 6
- keys: bfloat16 [4, 1024, 2048], P('dp', 'sp'), may hold values from -6 to 6
- values: bfloat16 [4, 1024, 2048], P('dp', 'sp'), may hold values from -6 to 6
- gate_totals: float32 [4, 1024, 32], P('dp', 'sp'), may hold values from -1024 to 0, as said below
- w_out: bfloat16 [2048, 2048], P(None, 'dp'), may hold values from -1 to 1
Outputs:
- mixed: bfloat16 [4, 1024, 2048], P('dp', 'sp')
Inputs may be any that keep to these rules, and one draw needn't show every extreme that they name: `gate_totals`: never rising along a sequence.
All inputs are finite; a program needn't handle non-finite values.
Results may differ from a plain program's by a relative error of at most 0.0053.
Values may be sent and summed in bfloat16 or wider, within the bound.
A program may use at most 64 MiB of HBM per device.

v0:
```python
import functools

import jax
import jax.numpy as jnp
from jax import lax
from jax.experimental import pallas as pl
from jax.experimental.pallas import tpu as pltpu
from jax.sharding import PartitionSpec as P

HEAD_DIM = 64
LANES = 128
W_CHUNKS = 16
MESH = pl.DeviceIdType.MESH


def attend(queries, key_rows, value_rows, totals):
    length = queries.shape[0]
    block_rows = min(length, 512)
    pieces = []
    for begin_row in range(0, length, block_rows):
        end_row = begin_row + block_rows
        scaled = queries[begin_row:end_row] * jnp.bfloat16(HEAD_DIM ** (-0.5))
        scores = jnp.einsum(
            "qhd,khd->hqk", scaled, key_rows[:end_row], preferred_element_type=jnp.float32
        )
        causal = jnp.arange(end_row)[None, :] <= (begin_row + jnp.arange(block_rows))[:, None]
        scores = jnp.where(
            causal[None],
            scores
            + jnp.transpose(totals[begin_row:end_row])[:, :, None]
            - jnp.transpose(totals[:end_row])[:, None, :],
            -jnp.inf,
        )
        biggest = jnp.max(scores, axis=-1, keepdims=True)
        expo = jnp.exp(scores - biggest)
        summed = jnp.sum(expo, axis=-1)
        weights = expo.astype(jnp.bfloat16)
        output = jnp.einsum(
            "hqk,khd->qhd", weights, value_rows[:end_row], preferred_element_type=jnp.float32
        )
        output = output / jnp.transpose(summed)[:, :, None]
        pieces.append(output.astype(jnp.bfloat16))
    return jnp.concatenate(pieces, axis=0).reshape(length, -1)


def general(queries, keys, values, gate_totals, w_out):
    moved = [
        lax.all_to_all(x, "sp", split_axis=2, concat_axis=1, tiled=True)
        for x in (queries, keys, values, gate_totals)
    ]
    length = moved[0].shape[1]
    heads = [x[0].reshape(length, -1, HEAD_DIM) for x in moved[:3]]
    attended = attend(heads[0], heads[1], heads[2], moved[3][0])[None]
    rows = lax.all_to_all(attended, "sp", split_axis=1, concat_axis=2, tiled=True)
    mixed = jnp.dot(
        rows[0],
        lax.all_gather(w_out, "dp", axis=1, tiled=True),
        preferred_element_type=jnp.float32,
    )
    return mixed.astype(jnp.bfloat16)[None]


def attend_rows(queries, parts, diagonal):
    rows = queries.shape[0]
    scaled = queries * jnp.bfloat16(HEAD_DIM ** -0.5)
    lane = lax.broadcasted_iota(jnp.int32, (rows, LANES), 1)
    outs, sums = [], []
    for h in range(2):
        mine = (lane < HEAD_DIM) if h == 0 else (lane >= HEAD_DIM)
        scores = []
        for at, (keys, _, gates) in enumerate(parts):
            head_keys = jnp.where(mine, keys, jnp.zeros_like(keys))
            score = lax.dot_general(
                scaled, head_keys, (((1,), (1,)), ((), ())), preferred_element_type=jnp.float32)
            score = score - gates[h:h + 1, :]
            if diagonal and at == len(parts) - 1:
                causal = lax.broadcasted_iota(jnp.int32, score.shape, 1) <= lax.broadcasted_iota(
                    jnp.int32, score.shape, 0)
                score = jnp.where(causal, score, -jnp.inf)
            scores.append(score)
        peak = functools.reduce(jnp.maximum, [jnp.max(x, axis=1, keepdims=True) for x in scores])
        expo = [jnp.exp(x - peak) for x in scores]
        total = sum(jnp.sum(x, axis=1, keepdims=True) for x in expo)
        out = sum(
            jnp.dot(x.astype(jnp.bfloat16), part[1], preferred_element_type=jnp.float32)
            for x, part in zip(expo, parts))
        outs.append(out / total)
        sums.append(peak + jnp.log(total))
    first = lane < HEAD_DIM
    return jnp.where(first, outs[0], outs[1]), jnp.where(first, sums[0], sums[1])


def kernel(n, ndp, q_ref, k_ref, v_ref, g_ref, w_ref, o_ref,
           qx, kx, vx, kz, vz, qz, gb, ob, held_o, held_l, part_o, part_l, got_o, got_l, att, wall, acc,
           x_send, x_recv, g_send, g_recv, own_sem, z_send, z_recv, po_send, po_recv, pl_send, pl_recv,
           o_send, o_recv, y_send, y_recv, wx_send, wx_recv, p_send, p_recv, f_send, f_recv):
    me = lax.axis_index("sp")
    x = lax.rem(me, 2)
    z = lax.div(me, 2)
    side = me + 1 - 2 * x
    me_dp = lax.axis_index("dp")
    core = lax.rem(me_dp, 2)
    row_y = lax.div(me_dp, 2)
    across = (1 - row_y) * 2 + core
    partner = row_y * 2 + 1 - core
    L = q_ref.shape[0]
    pairs = qx.shape[0]
    W = pairs * LANES
    w_rows, w_cols = w_ref.shape
    step_rows = w_rows // W_CHUNKS
    lent = W_CHUNKS // 8
    direct = W_CHUNKS - lent

    barrier = pltpu.get_barrier_semaphore()
    meets = {0: (1,), 1: (0, 2, 3), 2: (1, 3), 3: (1, 2)}
    for here, others in meets.items():
        @pl.when(z == here)
        def _(others=others):
            for other in others:
                pl.semaphore_signal(barrier, inc=1, device_id={"sp": other * 2 + x}, device_id_type=MESH)
    pl.semaphore_signal(barrier, inc=1, device_id={"sp": side}, device_id_type=MESH)
    for other in (partner, across):
        pl.semaphore_signal(barrier, inc=1, device_id={"dp": other}, device_id_type=MESH)
    for here, others in meets.items():
        @pl.when(z == here)
        def _(others=others):
            pl.semaphore_wait(barrier, len(others) + 3)

    def remote(src, dst, send, recv, **device):
        return pltpu.make_async_remote_copy(
            src_ref=src, dst_ref=dst, send_sem=send, recv_sem=recv, device_id=device, device_id_type=MESH)

    def rows_of(which):
        return pl.ds(pl.multiple_of(which * L, L), L)

    def lanes_of(which, p):
        return pl.ds(pl.multiple_of(which * W + p * LANES, LANES), LANES)

    bufs = ((q_ref, qx), (k_ref, kx), (v_ref, vx))

    def x_copy(a, p):
        src, dst = bufs[a]
        return remote(src.at[:, lanes_of(1 - x, p)], dst.at[p, rows_of(x), :],
                      x_send.at[a, p], x_recv.at[a, p], sp=side)

    def x_own(a, p):
        src, dst = bufs[a]
        return pltpu.make_async_copy(src.at[:, lanes_of(x, p)], dst.at[p, rows_of(x), :], own_sem.at[a, p])

    g_copy = remote(g_ref.at[1 - x], gb.at[me], g_send.at[0], g_recv.at[0], sp=side)
    g_own = pltpu.make_async_copy(g_ref.at[x], gb.at[me], g_recv.at[1])

    def chunk(s):
        if s < lent:
            at = s + direct * x
        elif s < direct:
            at = s
        else:
            at = (s - direct) + direct * (1 - x)
        return pl.ds(pl.multiple_of(at * step_rows, step_rows), step_rows)

    def y_copy(s):
        return remote(w_ref.at[chunk(s)], wall.at[me_dp, chunk(s)], y_send.at[s], y_recv.at[s], dp=across)

    def lend(s):
        return remote(wall.at[across, chunk(s)], wall.at[across, chunk(s)], wx_send.at[s], wx_recv.at[s], sp=side)

    def forward(s):
        return remote(wall.at[across, chunk(s)], wall.at[across, chunk(s)], f_send.at[s], f_recv.at[s], dp=partner)

    p_copy = remote(w_ref, wall.at[me_dp], p_send, p_recv, dp=partner)
    w_own = pltpu.make_async_copy(w_ref, wall.at[me_dp], own_sem.at[3, 0])

    for p in range(pairs):
        for a in range(3):
            x_copy(a, p).start()
        if p == 0:
            g_copy.start()
            for s in range(direct):
                y_copy(s).start()
            g_own.start()
        for a in range(3):
            x_own(a, p).start()
    p_copy.start()
    w_own.start()

    def pass_on(begin, end):
        for s in range(begin, end):
            if s < direct:
                y_copy(s).wait_recv()
            else:
                lend(s - direct).wait_recv()
            forward(s).start()
            if s < lent:
                lend(s).start()

    def arrived(p):
        for a in range(3):
            x_own(a, p).wait()
            x_copy(a, p).wait_recv()

    def to_z(src, dst, k, slot, p, target):
        return remote(src, dst, z_send.at[k, p], z_recv.at[slot, p], sp=target * 2 + x)

    def part_copies(k, slot, p, target):
        return (
            remote(part_o.at[k, p], got_o.at[slot, p], po_send.at[k, p], po_recv.at[slot, p], sp=target * 2 + x),
            remote(part_l.at[k, p], got_l.at[slot, p], pl_send.at[k, p], pl_recv.at[slot, p], sp=target * 2 + x),
        )

    def o_copy(p):
        return remote(ob.at[p, rows_of(1 - x), :], att.at[:, lanes_of(x, p)], o_send.at[p], o_recv.at[p], sp=side)

    def o_own(p):
        return pltpu.make_async_copy(ob.at[p, rows_of(x), :], att.at[:, lanes_of(x, p)], own_sem.at[3, 1 + p])

    def gates_of(block, p):
        return jnp.concatenate([gb[2 * block, p], gb[2 * block + 1, p]], axis=1)

    def finish(p, value):
        ob[p] = value.astype(jnp.bfloat16)
        o_copy(p).start()
        o_own(p).start()

    def share(p, k, slot, target, value, lse):
        part_o[k, p] = value.astype(jnp.bfloat16)
        turned = jnp.transpose(lse)
        part_l[k, p] = jnp.concatenate([turned[0:1], turned[HEAD_DIM:HEAD_DIM + 1]], axis=0)
        for copy in part_copies(k, slot, p, target):
            copy.start()

    def join(p, slots):
        outs, sums = [held_o[p]], [held_l[p]]
        for slot in slots:
            for copy in part_copies(0, slot, p, 0):
                copy.wait_recv()
            outs.append(got_o[slot, p].astype(jnp.float32))
            lse = got_l[slot, p]
            sums.append(jnp.transpose(jnp.concatenate(
                [jnp.broadcast_to(lse[h:h + 1], (HEAD_DIM, 2 * L)) for h in range(2)], axis=0)))
        peak = functools.reduce(jnp.maximum, sums)
        scale = [jnp.exp(s - peak) for s in sums]
        finish(p, sum(o * s for o, s in zip(outs, scale)) / sum(scale))

    def each(body, begin=0, end=None):
        def step(p, carry):
            body(p)
            return carry
        lax.fori_loop(begin, pairs if end is None else end, step, 0)

    def gates_here():
        g_own.wait()
        g_copy.wait_recv()

    def gates_up(target):
        return remote(gb.at[pl.ds(0, 2)], gb.at[pl.ds(0, 2)], g_send.at[1], g_recv.at[2], sp=target * 2 + x)

    half = pairs // 2

    @pl.when(z == 0)
    def _():
        gates_here()
        gates_up(1).start()
        def push(p):
            arrived(p)
            to_z(kx.at[p], kz.at[p], 0, 0, p, 1).start()
            to_z(vx.at[p], vz.at[p], 1, 1, p, 1).start()
        each(push)
        def work(p):
            finish(p, attend_rows(qx[p], [(kx[p], vx[p], gates_of(0, p))], True)[0])
        each(work)
        pass_on(0, lent)
        def left(p):
            to_z(kx.at[p], kz.at[p], 0, 0, p, 1).wait_send()
            to_z(vx.at[p], vz.at[p], 1, 1, p, 1).wait_send()
        each(left)
        gates_up(1).wait_send()

    @pl.when(z == 1)
    def _():
        gates_here()
        gates_up(0).wait_recv()
        def work(p):
            arrived(p)
            to_z(kx.at[p], kz.at[p], 0, 0, p, 0).wait_recv()
            to_z(vx.at[p], vz.at[p], 1, 1, p, 0).wait_recv()
            lower = (kz[p], vz[p], gates_of(0, p))
            own = (kx[p], vx[p], gates_of(1, p))
            finish(p, attend_rows(qx[p], [lower, own], True)[0])
            for k in range(2):
                to_z(qx.at[p], qz.at[k, p], 0, 2 + k, p, 0).wait_recv()
                share(p, k, 0, 2 + k, *attend_rows(qz[k, p], [lower, own], False))
        each(work, 0, half)
        pass_on(0, lent)
        each(work, half)
        def left(p):
            for k in range(2):
                for copy in part_copies(k, 0, p, 2 + k):
                    copy.wait_send()
        each(left)

    @pl.when(z == 2)
    def _():
        def push(p):
            arrived(p)
            to_z(qx.at[p], qz.at[0, p], 0, 2, p, 1).start()
        each(push)
        gates_here()
        def work(p):
            own = (kx[p], vx[p], gates_of(2, p))
            held_o[p], held_l[p] = attend_rows(qx[p], [own], True)
            to_z(qx.at[p], qz.at[0, p], 0, 2, p, 1).wait_recv()
            share(p, 1, 1, 3, *attend_rows(qz[0, p], [own], False))
        each(work)
        pass_on(0, lent)
        each(lambda p: join(p, (0,)))
        def left(p):
            to_z(qx.at[p], qz.at[0, p], 0, 2, p, 1).wait_send()
            for copy in part_copies(1, 1, p, 3):
                copy.wait_send()
        each(left)

    @pl.when(z == 3)
    def _():
        def push(p):
            arrived(p)
            to_z(qx.at[p], qz.at[1, p], 0, 3, p, 1).start()
            to_z(qx.at[p], qz.at[0, p], 1, 2, p, 2).start()
        each(push)
        gates_here()
        def work(p):
            held_o[p], held_l[p] = attend_rows(qx[p], [(kx[p], vx[p], gates_of(3, p))], True)
        each(work)
        pass_on(0, lent)
        each(lambda p: join(p, (0, 1)))
        def left(p):
            to_z(qx.at[p], qz.at[1, p], 0, 3, p, 1).wait_send()
            to_z(qx.at[p], qz.at[0, p], 1, 2, p, 2).wait_send()
        each(left)

    pass_on(lent, W_CHUNKS)

    def whole(p):
        o_own(p).wait()
        o_copy(p).wait_recv()
    each(whole)

    def columns(r):
        return pl.ds(pl.multiple_of(r * w_cols, LANES), w_cols)

    w_own.wait()
    o_ref[:, columns(me_dp)] = jnp.dot(
        att[...], wall[me_dp], preferred_element_type=jnp.float32).astype(o_ref.dtype)
    p_copy.wait_recv()
    o_ref[:, columns(partner)] = jnp.dot(
        att[...], wall[partner], preferred_element_type=jnp.float32).astype(o_ref.dtype)
    crossed = (1 - row_y) * 2 + 1 - core
    order = list(range(lent)) + list(range(direct, W_CHUNKS)) + list(range(lent, direct))
    for at, s in enumerate(order):
        left = att[:, chunk(s)]
        for which, r in ((0, across), (1, crossed)):
            if which:
                forward(s).wait_recv()
            part = jnp.dot(left, wall[r, chunk(s)], preferred_element_type=jnp.float32)
            if at > 0:
                part = acc[which] + part
            if at < W_CHUNKS - 1:
                acc[which] = part
            else:
                o_ref[:, columns(r)] = part.astype(o_ref.dtype)

    p_copy.wait_send()
    g_copy.wait_send()
    def sent(p):
        o_copy(p).wait_send()
        for a in range(3):
            x_copy(a, p).wait_send()
    each(sent)
    for s in range(W_CHUNKS):
        if s < direct:
            y_copy(s).wait_send()
        if s < lent:
            lend(s).wait_send()
        forward(s).wait_send()


def fused(n, ndp, queries, keys, values, gate_totals, w_out):
    L, model = queries.shape[1], queries.shape[2]
    heads = gate_totals.shape[2] // 2
    pairs = heads * HEAD_DIM // LANES
    gates = jnp.transpose(gate_totals[0]).reshape(2, pairs, 2, L)
    w_rows, w_cols = w_out.shape
    bf16, f32 = jnp.bfloat16, jnp.float32
    dma = pltpu.SemaphoreType.DMA
    block = (pairs, 2 * L, LANES)
    out = pl.pallas_call(
        functools.partial(kernel, n, ndp),
        out_shape=jax.ShapeDtypeStruct((L, w_cols * ndp), bf16),
        in_specs=[pl.BlockSpec(memory_space=pl.ANY)] * 5,
        out_specs=pl.BlockSpec(memory_space=pltpu.VMEM),
        scratch_shapes=[
            *[pltpu.VMEM(block, bf16)] * 5,
            pltpu.VMEM((2,) + block, bf16),
            pltpu.VMEM((n, pairs, 2, L), f32),
            pltpu.VMEM(block, bf16),
            pltpu.VMEM(block, f32),
            pltpu.VMEM(block, f32),
            pltpu.VMEM((2,) + block, bf16),
            pltpu.VMEM((2, pairs, 2, 2 * L), f32),
            pltpu.VMEM((2,) + block, bf16),
            pltpu.VMEM((2, pairs, 2, 2 * L), f32),
            pltpu.VMEM((L, model), bf16),
            pltpu.VMEM((ndp, w_rows, w_cols), bf16),
            pltpu.VMEM((2, L, w_cols), f32),
            dma((3, pairs)), dma((3, pairs)), dma((2,)), dma((3,)), dma((4, pairs + 1)),
            dma((2, pairs)), dma((4, pairs)),
            dma((2, pairs)), dma((2, pairs)), dma((2, pairs)), dma((2, pairs)),
            dma((pairs,)), dma((pairs,)),
            dma((W_CHUNKS,)), dma((W_CHUNKS,)), dma((W_CHUNKS,)), dma((W_CHUNKS,)), dma, dma,
            dma((W_CHUNKS,)), dma((W_CHUNKS,)),
        ],
        compiler_params=pltpu.CompilerParams(
            collective_id=0, has_side_effects=True, vmem_limit_bytes=67043328),
        name="fused_attention",
    )(queries[0], keys[0], values[0], gates, w_out)
    return out[None]


def solution(mesh):
    n, ndp = mesh.shape["sp"], mesh.shape["dp"]

    def local(queries, keys, values, gate_totals, w_out):
        fits = n == 8 and ndp == 4 and queries.shape[1] % LANES == 0
        if fits:
            return fused(n, ndp, queries, keys, values, gate_totals, w_out)
        return general(queries, keys, values, gate_totals, w_out)

    placed = (P("dp", "sp", None),) * 4 + (P(None, "dp"),)
    return jax.shard_map(
        local, mesh=mesh, in_specs=placed, out_specs=P("dp", "sp", None), check_vma=False)
```

profile of v0, /device:TPU:11, one launch (start us, length us, event | category | flops | bytes accessed | tf_op | source)
XLA Modules:
  0.0 52.9 jit_solution(12733717579833328101)
XLA Ops:
  0.0 51.0 %fused_attention.1 = bf16[128,2048]{1,0:T(8,128)(2,1)} custom-call(bf16[128,2048]{1,0:T(8,128)(2,1)} %bitcast.10, bf16[128,2048]{1,0:T(8,128)(2,1)} %bitcast.11, bf16[128,2048]{1,0:T(8,128)(2,1)} %bitcast.12, f32[2,8,2,128]{3,2,1,0:T(2,128)} %bitcast.13, bf16[2048,512]{1,0:T(8,128)(2,1)} %w_ref.1), custom_call_target="tpu_custom_call" | custom-call | tf_op jit(solution)/shard_map/fused_attention/pallas_call | solution.py:396
  51.0 1.9 %copy.7 = bf16[1,128,2048]{2,1,0:T(8,128)(2,1)} copy(bf16[1,128,2048]{2,1,0:T(8,128)(2,1)} %bitcast.9) | data formatting | bytes 1048576
where the time goes:
time: 53.1 us; the launch traced here: 52.9 us
  Pallas kernels  51 us (96%)
  local copies, waits for them, and re-layouts  1.88 us (4%)
    pallas_call x1, Pallas kernels, fused(): pl.pallas_call(functools.partial(kernel, n, ndp), out_shape=jax.ShapeDtyp...  51 us
    unnamed x1, local copies, waits for them, and re-layouts  1.88 us

commit v1 on v0

--- a/solution.py
+++ b/solution.py
@@ -92,7 +92,7 @@
 
 def kernel(n, ndp, q_ref, k_ref, v_ref, g_ref, w_ref, o_ref,
            qx, kx, vx, kz, vz, qz, gb, ob, held_o, held_l, part_o, part_l, got_o, got_l, att, wall, acc,
-           x_send, x_recv, g_send, g_recv, own_sem, z_send, z_recv, po_send, po_recv, pl_send, pl_recv,
+           x_send, x_recv, g_send, g_recv, own_sem, w_sem, z_send, z_recv, po_send, po_recv, pl_send, pl_recv,
            o_send, o_recv, y_send, y_recv, wx_send, wx_recv, p_send, p_recv, f_send, f_recv):
     me = lax.axis_index("sp")
     x = lax.rem(me, 2)
@@ -106,10 +106,9 @@
     L = q_ref.shape[0]
     pairs = qx.shape[0]
     W = pairs * LANES
-    w_rows, w_cols = w_ref.shape
-    step_rows = w_rows // W_CHUNKS
-    lent = W_CHUNKS // 8
-    direct = W_CHUNKS - lent
+    w_cols = w_ref.shape[3]
+    units = 3 * pairs // 4
+    quarter = pairs // 4
 
     barrier = pltpu.get_barrier_semaphore()
     meets = {0: (1,), 1: (0, 2, 3), 2: (1, 3), 3: (1, 2)}
@@ -136,6 +135,9 @@
     def lanes_of(which, p):
         return pl.ds(pl.multiple_of(which * W + p * LANES, LANES), LANES)
 
+    def half_of(which):
+        return pl.ds(pl.multiple_of(which * LANES, LANES), LANES)
+
     bufs = ((q_ref, qx), (k_ref, kx), (v_ref, vx))
 
     def x_copy(a, p):
@@ -150,57 +152,128 @@
     g_copy = remote(g_ref.at[1 - x], gb.at[me], g_send.at[0], g_recv.at[0], sp=side)
     g_own = pltpu.make_async_copy(g_ref.at[x], gb.at[me], g_recv.at[1])
 
-    def chunk(s):
-        if s < lent:
-            at = s + direct * x
-        elif s < direct:
-            at = s
-        else:
-            at = (s - direct) + direct * (1 - x)
-        return pl.ds(pl.multiple_of(at * step_rows, step_rows), step_rows)
-
-    def y_copy(s):
-        return remote(w_ref.at[chunk(s)], wall.at[me_dp, chunk(s)], y_send.at[s], y_recv.at[s], dp=across)
-
-    def lend(s):
-        return remote(wall.at[across, chunk(s)], wall.at[across, chunk(s)], wx_send.at[s], wx_recv.at[s], sp=side)
-
-    def forward(s):
-        return remote(wall.at[across, chunk(s)], wall.at[across, chunk(s)], f_send.at[s], f_recv.at[s], dp=partner)
+    def z_own(a, dst, k, slot, p, target):
+        src = bufs[a][0]
+        return remote(src.at[:, lanes_of(x, p)], dst.at[rows_of(x), :],
+                      z_send.at[k, x, p], z_recv.at[slot, x, p], sp=target * 2 + x)
+
+    def z_side(a, dst, k, slot, p, target):
+        src = bufs[a][1]
+        return remote(src.at[p, rows_of(1 - x), :], dst.at[rows_of(1 - x), :],
+                      z_send.at[k, 1 - x, p], z_recv.at[slot, 1 - x, p], sp=target * 2 + x)
+
+    def z_arrived(a, dst, slot, p):
+        z_own(a, dst, 0, slot, p, 0).wait_recv()
+        z_side(a, dst, 0, slot, p, 0).wait_recv()
+
+    def z_sent(a, dst, k, slot, p, target):
+        z_own(a, dst, k, slot, p, target).wait_send()
+        z_side(a, dst, k, slot, p, target).wait_send()
+
+    def up_k(p):
+        return (1, kz.at[p], 0, 0, p, 1)
+
+    def up_v(p):
+        return (2, vz.at[p], 1, 1, p, 1)
+
+    def down_two(p):
+        return (0, qz.at[0, p], 0, 2, p, 1)
+
+    def down_three(p):
+        return (0, qz.at[1, p], 0, 3, p, 1)
+
+    def down_near(p):
+        return (0, qz.at[0, p], 1, 2, p, 2)
+
+    lent = [2 * j for j in range(quarter)]
+    order = []
+    for j in range(pairs // 4):
+        order += [pairs // 2 + j, j]
+    order += list(range(pairs // 4, pairs // 2))
+
+    def pair_of(u):
+        return order[u] + quarter * x if u in lent else order[u]
+
+    def loan_of(j):
+        return pairs // 2 + j + quarter * (1 - x)
+
+    def w_of(r, q):
+        return wall.at[r, :, q]
+
+    def y_copy(u):
+        return remote(w_ref.at[:, pair_of(u)], w_of(me_dp, pair_of(u)), y_send.at[u], y_recv.at[u], dp=across)
+
+    def lend(j):
+        q = pair_of(lent[j])
+        return remote(w_of(across, q), w_of(across, q), wx_send.at[j], wx_recv.at[j], sp=side)
+
+    def borrowed(j):
+        q = loan_of(j)
+        return remote(w_of(across, q), w_of(across, q), wx_send.at[j], wx_recv.at[j], sp=side)
+
+    def forward(q):
+        return remote(w_of(across, q), w_of(across, q), f_send.at[q], f_recv.at[q], dp=partner)
 
     p_copy = remote(w_ref, wall.at[me_dp], p_send, p_recv, dp=partner)
-    w_own = pltpu.make_async_copy(w_ref, wall.at[me_dp], own_sem.at[3, 0])
-
+    w_own = pltpu.make_async_copy(w_ref, wall.at[me_dp], w_sem)
+
+    g_copy.start()
+    g_own.start()
+
+    @pl.when(z < 2)
+    def _():
+        for p in range(pairs):
+            for a in (1, 2, 0):
+                x_copy(a, p).start()
+
+    @pl.when(z >= 2)
+    def _():
+        for p in range(pairs):
+            x_copy(0, p).start()
+        for p in range(pairs):
+            for a in (1, 2):
+                x_copy(a, p).start()
+
+    ahead = min(2, pairs)
+
+    @pl.when(z == 0)
+    def _():
+        for p in range(ahead):
+            z_own(*up_k(p)).start()
+            z_own(*up_v(p)).start()
+
+    @pl.when(z == 2)
+    def _():
+        for p in range(ahead):
+            z_own(*down_two(p)).start()
+
+    @pl.when(z == 3)
+    def _():
+        for p in range(ahead):
+            z_own(*down_three(p)).start()
+            z_own(*down_near(p)).start()
+
+    for u in range(units):
+        y_copy(u).start()
     for p in range(pairs):
-        for a in range(3):
-            x_copy(a, p).start()
-        if p == 0:
-            g_copy.start()
-            for s in range(direct):
-                y_copy(s).start()
-            g_own.start()
         for a in range(3):
             x_own(a, p).start()
     p_copy.start()
     w_own.start()
 
-    def pass_on(begin, end):
-        for s in range(begin, end):
-            if s < direct:
-                y_copy(s).wait_recv()
-            else:
-                lend(s - direct).wait_recv()
-            forward(s).start()
-            if s < lent:
-                lend(s).start()
-
-    def arrived(p):
-        for a in range(3):
-            x_own(a, p).wait()
-            x_copy(a, p).wait_recv()
-
-    def to_z(src, dst, k, slot, p, target):
-        return remote(src, dst, z_send.at[k, p], z_recv.at[slot, p], sp=target * 2 + x)
+    def pass_on(u):
+        y_copy(u).wait_recv()
+        if u in lent:
+            lend(lent.index(u)).start()
+        forward(pair_of(u)).start()
+
+    def pass_loan(j):
+        borrowed(j).wait_recv()
+        forward(loan_of(j)).start()
+
+    def arrived(a, p):
+        x_own(a, p).wait()
+        x_copy(a, p).wait_recv()
 
     def part_copies(k, slot, p, target):
         return (
@@ -209,10 +282,7 @@
         )
 
     def o_copy(p):
-        return remote(ob.at[p, rows_of(1 - x), :], att.at[:, lanes_of(x, p)], o_send.at[p], o_recv.at[p], sp=side)
-
-    def o_own(p):
-        return pltpu.make_async_copy(ob.at[p, rows_of(x), :], att.at[:, lanes_of(x, p)], own_sem.at[3, 1 + p])
+        return remote(ob.at[p, rows_of(1 - x), :], att.at[p, :, half_of(x)], o_send.at[p], o_recv.at[p], sp=side)
 
     def gates_of(block, p):
         return jnp.concatenate([gb[2 * block, p], gb[2 * block + 1, p]], axis=1)
@@ -220,7 +290,7 @@
     def finish(p, value):
         ob[p] = value.astype(jnp.bfloat16)
         o_copy(p).start()
-        o_own(p).start()
+        att[p, :, half_of(x)] = ob[p, rows_of(x), :]
 
     def share(p, k, slot, target, value, lse):
         part_o[k, p] = value.astype(jnp.bfloat16)
@@ -255,44 +325,140 @@
     def gates_up(target):
         return remote(gb.at[pl.ds(0, 2)], gb.at[pl.ds(0, 2)], g_send.at[1], g_recv.at[2], sp=target * 2 + x)
 
-    half = pairs // 2
+    def passing(p, first, every):
+        for u in range(units):
+            at = first + every * u
+            if at < pairs:
+                @pl.when(p == at)
+                def _(u=u):
+                    pass_on(u)
+
+    def passed(first, every):
+        return [u for u in range(units) if first + every * u < pairs]
+
+    def pass_rest(first, every):
+        for u in range(len(passed(first, every)), units):
+            pass_on(u)
+
+    def push(p, makers):
+        @pl.when(p + ahead < pairs)
+        def _():
+            for make in makers:
+                z_own(*make(p + ahead)).start()
+        for make in makers:
+            if make in (up_v, up_k):
+                arrived(make(p)[0], p)
+            z_side(*make(p)).start()
 
     @pl.when(z == 0)
     def _():
         gates_here()
         gates_up(1).start()
-        def push(p):
-            arrived(p)
-            to_z(kx.at[p], kz.at[p], 0, 0, p, 1).start()
-            to_z(vx.at[p], vz.at[p], 1, 1, p, 1).start()
-        each(push)
         def work(p):
+            push(p, (up_k, up_v))
+            arrived(0, p)
             finish(p, attend_rows(qx[p], [(kx[p], vx[p], gates_of(0, p))], True)[0])
+            passing(p, 3, 3)
         each(work)
-        pass_on(0, lent)
-        def left(p):
-            to_z(kx.at[p], kz.at[p], 0, 0, p, 1).wait_send()
-            to_z(vx.at[p], vz.at[p], 1, 1, p, 1).wait_send()
-        each(left)
-        gates_up(1).wait_send()
+        pass_rest(3, 3)
 
     @pl.when(z == 1)
     def _():
         gates_here()
         gates_up(0).wait_recv()
         def work(p):
-            arrived(p)
-            to_z(kx.at[p], kz.at[p], 0, 0, p, 0).wait_recv()
-            to_z(vx.at[p], vz.at[p], 1, 1, p, 0).wait_recv()
+            arrived(1, p)
+            arrived(2, p)
+            z_arrived(1, kz.at[p], 0, p)
+            z_arrived(2, vz.at[p], 1, p)
             lower = (kz[p], vz[p], gates_of(0, p))
             own = (kx[p], vx[p], gates_of(1, p))
+            for k in (1, 0):
+                z_arrived(0, qz.at[k, p], 2 + k, p)
+                share(p, k, 0, 2 + k, *attend_rows(qz[k, p], [lower, own], False))
+            arrived(0, p)
             finish(p, attend_rows(qx[p], [lower, own], True)[0])
-            for k in range(2):
-                to_z(qx.at[p], qz.at[k, p], 0, 2 + k, p, 0).wait_recv()
-                share(p, k, 0, 2 + k, *attend_rows(qz[k, p], [lower, own], False))
-        each(work, 0, half)
-        pass_on(0, lent)
-        each(work, half)
+            passing(p, 1, 2)
+        each(work)
+        pass_rest(1, 2)
+
+    @pl.when(z == 2)
+    def _():
+        def pushes(p):
+            arrived(0, p)
+            push(p, (down_two,))
+        each(pushes)
+        gates_here()
+        lag = min(2, pairs)
+        def work(p):
+            arrived(1, p)
+            arrived(2, p)
+            own = (kx[p], vx[p], gates_of(2, p))
+            z_arrived(0, qz.at[0, p], 2, p)
+            share(p, 1, 1, 3, *attend_rows(qz[0, p], [own], False))
+            held_o[p], held_l[p] = attend_rows(qx[p], [own], True)
+            @pl.when(p >= lag)
+            def _():
+                join(p - lag, (0,))
+            passing(p, 1, 2)
+        each(work)
+        each(lambda p: join(p, (0,)), pairs - lag)
+        pass_rest(1, 2)
+
+    @pl.when(z == 3)
+    def _():
+        def pushes(p):
+            arrived(0, p)
+            push(p, (down_three, down_near))
+        each(pushes)
+        gates_here()
+        def work(p):
+            arrived(1, p)
+            arrived(2, p)
+            held_o[p], held_l[p] = attend_rows(qx[p], [(kx[p], vx[p], gates_of(3, p))], True)
+            passing(p, 1, 4)
+        each(work)
+        def last(p):
+            join(p, (0, 1))
+            for u in range(len(passed(1, 4)), units):
+                @pl.when(p == 2 * (u - len(passed(1, 4))))
+                def _(u=u):
+                    pass_on(u)
+        each(last)
+
+    for j in range(quarter):
+        pass_loan(j)
+
+    w_own.wait()
+    p_copy.wait_recv()
+    steps = [0, 1, 4, 2, 5, 6, 3, 7] if pairs == 8 else list(range(pairs))
+    for at, q in enumerate(steps):
+        o_copy(q).wait_recv()
+        forward(q).wait_recv()
+        left = att[q]
+        for r in range(ndp):
+            columns = slice(r * w_cols, (r + 1) * w_cols)
+            part = jnp.dot(left, wall[r, :, q].reshape(2 * LANES, w_cols), preferred_element_type=jnp.float32)
+            if at > 0:
+                part = acc[:, columns] + part
+            if at < pairs - 1:
+                acc[:, columns] = part
+            else:
+                o_ref[:, columns] = part.astype(o_ref.dtype)
+
+    p_copy.wait_send()
+    g_copy.wait_send()
+
+    @pl.when(z == 0)
+    def _():
+        def left(p):
+            z_sent(*up_k(p))
+            z_sent(*up_v(p))
+        each(left)
+        gates_up(1).wait_send()
+
+    @pl.when(z == 1)
+    def _():
         def left(p):
             for k in range(2):
                 for copy in part_copies(k, 0, p, 2 + k):
@@ -301,87 +467,29 @@
 
     @pl.when(z == 2)
     def _():
-        def push(p):
-            arrived(p)
-            to_z(qx.at[p], qz.at[0, p], 0, 2, p, 1).start()
-        each(push)
-        gates_here()
-        def work(p):
-            own = (kx[p], vx[p], gates_of(2, p))
-            held_o[p], held_l[p] = attend_rows(qx[p], [own], True)
-            to_z(qx.at[p], qz.at[0, p], 0, 2, p, 1).wait_recv()
-            share(p, 1, 1, 3, *attend_rows(qz[0, p], [own], False))
-        each(work)
-        pass_on(0, lent)
-        each(lambda p: join(p, (0,)))
         def left(p):
-            to_z(qx.at[p], qz.at[0, p], 0, 2, p, 1).wait_send()
+            z_sent(*down_two(p))
             for copy in part_copies(1, 1, p, 3):
                 copy.wait_send()
         each(left)
 
     @pl.when(z == 3)
     def _():
-        def push(p):
-            arrived(p)
-            to_z(qx.at[p], qz.at[1, p], 0, 3, p, 1).start()
-            to_z(qx.at[p], qz.at[0, p], 1, 2, p, 2).start()
-        each(push)
-        gates_here()
-        def work(p):
-            held_o[p], held_l[p] = attend_rows(qx[p], [(kx[p], vx[p], gates_of(3, p))], True)
-        each(work)
-        pass_on(0, lent)
-        each(lambda p: join(p, (0, 1)))
         def left(p):
-            to_z(qx.at[p], qz.at[1, p], 0, 3, p, 1).wait_send()
-            to_z(qx.at[p], qz.at[0, p], 1, 2, p, 2).wait_send()
+            z_sent(*down_three(p))
+            z_sent(*down_near(p))
         each(left)
 
-    pass_on(lent, W_CHUNKS)
-
-    def whole(p):
-        o_own(p).wait()
-        o_copy(p).wait_recv()
-    each(whole)
-
-    def columns(r):
-        return pl.ds(pl.multiple_of(r * w_cols, LANES), w_cols)
-
-    w_own.wait()
-    o_ref[:, columns(me_dp)] = jnp.dot(
-        att[...], wall[me_dp], preferred_element_type=jnp.float32).astype(o_ref.dtype)
-    p_copy.wait_recv()
-    o_ref[:, columns(partner)] = jnp.dot(
-        att[...], wall[partner], preferred_element_type=jnp.float32).astype(o_ref.dtype)
-    crossed = (1 - row_y) * 2 + 1 - core
-    order = list(range(lent)) + list(range(direct, W_CHUNKS)) + list(range(lent, direct))
-    for at, s in enumerate(order):
-        left = att[:, chunk(s)]
-        for which, r in ((0, across), (1, crossed)):
-            if which:
-                forward(s).wait_recv()
-            part = jnp.dot(left, wall[r, chunk(s)], preferred_element_type=jnp.float32)
-            if at > 0:
-                part = acc[which] + part
-            if at < W_CHUNKS - 1:
-                acc[which] = part
-            else:
-                o_ref[:, columns(r)] = part.astype(o_ref.dtype)
-
-    p_copy.wait_send()
-    g_copy.wait_send()
     def sent(p):
         o_copy(p).wait_send()
+        forward(p).wait_send()
         for a in range(3):
             x_copy(a, p).wait_send()
     each(sent)
-    for s in range(W_CHUNKS):
-        if s < direct:
-            y_copy(s).wait_send()
-        if s < lent:
-            lend(s).wait_send()
-        forward(s).wait_send()
+    for u in range(units):
+        y_copy(u).wait_send()
+    for j in range(quarter):
+        lend(j).wait_send()
 
 
 def fused(n, ndp, queries, keys, values, gate_totals, w_out):
@@ -389,10 +497,12 @@
     heads = gate_totals.shape[2] // 2
     pairs = heads * HEAD_DIM // LANES
     gates = jnp.transpose(gate_totals[0]).reshape(2, pairs, 2, L)
-    w_rows, w_cols = w_out.shape
+    w_cols = w_out.shape[1]
+    weights = w_out.reshape(2, pairs, LANES, w_cols)
     bf16, f32 = jnp.bfloat16, jnp.float32
     dma = pltpu.SemaphoreType.DMA
     block = (pairs, 2 * L, LANES)
+    units, quarter = 3 * pairs // 4, pairs // 4
     out = pl.pallas_call(
         functools.partial(kernel, n, ndp),
         out_shape=jax.ShapeDtypeStruct((L, w_cols * ndp), bf16),
@@ -409,20 +519,20 @@
             pltpu.VMEM((2, pairs, 2, 2 * L), f32),
             pltpu.VMEM((2,) + block, bf16),
             pltpu.VMEM((2, pairs, 2, 2 * L), f32),
-            pltpu.VMEM((L, model), bf16),
-            pltpu.VMEM((ndp, w_rows, w_cols), bf16),
-            pltpu.VMEM((2, L, w_cols), f32),
-            dma((3, pairs)), dma((3, pairs)), dma((2,)), dma((3,)), dma((4, pairs + 1)),
-            dma((2, pairs)), dma((4, pairs)),
+            pltpu.VMEM((pairs, L, 2 * LANES), bf16),
+            pltpu.VMEM((ndp, 2, pairs, LANES, w_cols), bf16),
+            pltpu.VMEM((L, ndp * w_cols), f32),
+            dma((3, pairs)), dma((3, pairs)), dma((2,)), dma((3,)), dma((3, pairs)), dma,
+            dma((2, 2, pairs)), dma((4, 2, pairs)),
             dma((2, pairs)), dma((2, pairs)), dma((2, pairs)), dma((2, pairs)),
             dma((pairs,)), dma((pairs,)),
-            dma((W_CHUNKS,)), dma((W_CHUNKS,)), dma((W_CHUNKS,)), dma((W_CHUNKS,)), dma, dma,
-            dma((W_CHUNKS,)), dma((W_CHUNKS,)),
+            dma((units,)), dma((units,)), dma((quarter,)), dma((quarter,)), dma, dma,
+            dma((pairs,)), dma((pairs,)),
         ],
         compiler_params=pltpu.CompilerParams(
             collective_id=0, has_side_effects=True, vmem_limit_bytes=67043328),
         name="fused_attention",
-    )(queries[0], keys[0], values[0], gates, w_out)
+    )(queries[0], keys[0], values[0], gates, weights)
     return out[None]
 
 
@@ -430,7 +540,7 @@
     n, ndp = mesh.shape["sp"], mesh.shape["dp"]
 
     def local(queries, keys, values, gate_totals, w_out):
-        fits = n == 8 and ndp == 4 and queries.shape[1] % LANES == 0
+        fits = n == 8 and ndp == 4 and queries.shape[1] % LANES == 0 and queries.shape[2] % (8 * LANES) == 0
         if fits:
             return fused(n, ndp, queries, keys, values, gate_totals, w_out)
         return general(queries, keys, values, gate_totals, w_out)

time: 53.1 us -> 47.6 us (0.90)
  Pallas kernels: 51 us -> 45.5 us
    pallas_call x1, Pallas kernels: 51 us -> 45.5 us  [fused(): pl.pallas_call(functools.partial(kernel, n, ndp), out_shape=jax.ShapeDtyp...]
where the time goes in v1:
time: 47.6 us; the launch traced here: 47.4 us
  Pallas kernels  45.5 us (96%)
  local copies, waits for them, and re-layouts  1.88 us (4%)
    pallas_call x1, Pallas kernels, fused(): pl.pallas_call(functools.partial(kernel, n, ndp), out_shape=jax.ShapeDtyp...  45.5 us
    unnamed x1, local copies, waits for them, and re-layouts  1.88 us

profile of v1, /device:TPU:11, one launch (start us, length us, event | category | flops | bytes accessed | tf_op | source)
XLA Modules:
  0.0 47.4 jit_solution(8298597130926932826)
XLA Ops:
  0.0 45.5 %fused_attention.1 = bf16[128,2048]{1,0:T(8,128)(2,1)} custom-call(bf16[128,2048]{1,0:T(8,128)(2,1)} %bitcast.12, bf16[128,2048]{1,0:T(8,128)(2,1)} %bitcast.13, bf16[128,2048]{1,0:T(8,128)(2,1)} %bitcast.14, f32[2,8,2,128]{3,2,1,0:T(2,128)} %bitcast.15, bf16[2,8,128,512]{3,2,1,0:T(8,128)(2,1)} %bitcast.10), custom_call_target="tpu_custom_call" | custom-call | tf_op jit(solution)/shard_map/fused_attention/pallas_call | solution.py:506
  45.5 1.9 %copy.7 = bf16[1,128,2048]{2,1,0:T(8,128)(2,1)} copy(bf16[1,128,2048]{2,1,0:T(8,128)(2,1)} %bitcast.11) | data formatting | bytes 1048576

commit v2 on v1

v2 whole, which is shorter than its diff:
```python
import functools

import jax
import jax.numpy as jnp
from jax import lax
from jax.experimental import pallas as pl
from jax.experimental.pallas import tpu as pltpu
from jax.sharding import PartitionSpec as P

HEAD_DIM = 64
LANES = 128
W_CHUNKS = 16
MESH = pl.DeviceIdType.MESH


def attend(queries, key_rows, value_rows, totals):
    length = queries.shape[0]
    block_rows = min(length, 512)
    pieces = []
    for begin_row in range(0, length, block_rows):
        end_row = begin_row + block_rows
        scaled = queries[begin_row:end_row] * jnp.bfloat16(HEAD_DIM ** (-0.5))
        scores = jnp.einsum(
            "qhd,khd->hqk", scaled, key_rows[:end_row], preferred_element_type=jnp.float32
        )
        causal = jnp.arange(end_row)[None, :] <= (begin_row + jnp.arange(block_rows))[:, None]
        scores = jnp.where(
            causal[None],
            scores
            + jnp.transpose(totals[begin_row:end_row])[:, :, None]
            - jnp.transpose(totals[:end_row])[:, None, :],
            -jnp.inf,
        )
        biggest = jnp.max(scores, axis=-1, keepdims=True)
        expo = jnp.exp(scores - biggest)
        summed = jnp.sum(expo, axis=-1)
        weights = expo.astype(jnp.bfloat16)
        output = jnp.einsum(
            "hqk,khd->qhd", weights, value_rows[:end_row], preferred_element_type=jnp.float32
        )
        output = output / jnp.transpose(summed)[:, :, None]
        pieces.append(output.astype(jnp.bfloat16))
    return jnp.concatenate(pieces, axis=0).reshape(length, -1)


def general(queries, keys, values, gate_totals, w_out):
    moved = [
        lax.all_to_all(x, "sp", split_axis=2, concat_axis=1, tiled=True)
        for x in (queries, keys, values, gate_totals)
    ]
    length = moved[0].shape[1]
    heads = [x[0].reshape(length, -1, HEAD_DIM) for x in moved[:3]]
    attended = attend(heads[0], heads[1], heads[2], moved[3][0])[None]
    rows = lax.all_to_all(attended, "sp", split_axis=1, concat_axis=2, tiled=True)
    mixed = jnp.dot(
        rows[0],
        lax.all_gather(w_out, "dp", axis=1, tiled=True),
        preferred_element_type=jnp.float32,
    )
    return mixed.astype(jnp.bfloat16)[None]


def attend_rows(queries, parts, diagonal):
    rows = queries.shape[0]
    scaled = queries * jnp.bfloat16(HEAD_DIM ** -0.5)
    lane = lax.broadcasted_iota(jnp.int32, (rows, LANES), 1)
    outs, sums = [], []
    for h in range(2):
        mine = (lane < HEAD_DIM) if h == 0 else (lane >= HEAD_DIM)
        scores = []
        for at, (keys, _, gates) in enumerate(parts):
            head_keys = jnp.where(mine, keys, jnp.zeros_like(keys))
            score = lax.dot_general(
                scaled, head_keys, (((1,), (1,)), ((), ())), preferred_element_type=jnp.float32)
            score = score - gates[h:h + 1, :]
            if diagonal and at == len(parts) - 1:
                causal = lax.broadcasted_iota(jnp.int32, score.shape, 1) <= lax.broadcasted_iota(
                    jnp.int32, score.shape, 0)
                score = jnp.where(causal, score, -jnp.inf)
            scores.append(score)
        peak = functools.reduce(jnp.maximum, [jnp.max(x, axis=1, keepdims=True) for x in scores])
        expo = [jnp.exp(x - peak) for x in scores]
        total = sum(jnp.sum(x, axis=1, keepdims=True) for x in expo)
        out = sum(
            jnp.dot(x.astype(jnp.bfloat16), part[1], preferred_element_type=jnp.float32)
            for x, part in zip(expo, parts))
        outs.append(out / total)
        sums.append(peak + jnp.log(total))
    first = lane < HEAD_DIM
    return jnp.where(first, outs[0], outs[1]), jnp.where(first, sums[0], sums[1])


def kernel(n, ndp, q_ref, k_ref, v_ref, g_ref, w_ref, o_ref,
           qx, kvx, zin, gb, ob, held_o, held_l, part_o, part_l, got_o, got_l, att, wall, acc,
           q_recv, kv_recv, x_send, g_send, g_recv, z_send, z_recv, po_send, po_recv, pl_send, pl_recv,
           o_send, o_recv, y_recv, yh_recv, wx_recv, wz_recv, w_recv, w_send):
    me = lax.axis_index("sp")
    x = lax.rem(me, 2)
    z = lax.div(me, 2)
    side = me + 1 - 2 * x
    me_dp = lax.axis_index("dp")
    core = lax.rem(me_dp, 2)
    row_y = lax.div(me_dp, 2)
    across = (1 - row_y) * 2 + core
    partner = row_y * 2 + 1 - core
    L = q_ref.shape[0]
    pairs = qx.shape[0]
    W = pairs * LANES
    w_cols = w_ref.shape[3]
    quarter = pairs // 4
    units = quarter * 2
    step_z = quarter // 2
    odd = lax.rem(z, 2)
    other_z = z + 1 - 2 * odd

    barrier = pltpu.get_barrier_semaphore()
    meets = {0: (1,), 1: (0, 2, 3), 2: (1, 3), 3: (1, 2)}
    for here, others in meets.items():
        @pl.when(z == here)
        def _(others=others):
            for other in others:
                pl.semaphore_signal(barrier, inc=1, device_id={"sp": other * 2 + x}, device_id_type=MESH)
    pl.semaphore_signal(barrier, inc=1, device_id={"sp": side}, device_id_type=MESH)
    for other in (partner, across):
        pl.semaphore_signal(barrier, inc=1, device_id={"dp": other}, device_id_type=MESH)
    for here, others in meets.items():
        @pl.when(z == here)
        def _(others=others):
            pl.semaphore_wait(barrier, len(others) + 3)

    def remote(src, dst, send, recv, **device):
        return pltpu.make_async_remote_copy(
            src_ref=src, dst_ref=dst, send_sem=send, recv_sem=recv, device_id=device, device_id_type=MESH)

    def rows_of(which):
        return pl.ds(pl.multiple_of(which * L, L), L)

    def lanes_of(which, p):
        return pl.ds(pl.multiple_of(which * W + p * LANES, LANES), LANES)

    def half_of(which):
        return pl.ds(pl.multiple_of(which * LANES, LANES), LANES)

    def landing(a, p):
        return qx.at[p] if a == 0 else kvx.at[p, a - 1]

    refs = (q_ref, k_ref, v_ref)

    def x_sem(a, p):
        return q_recv.at[p] if a == 0 else kv_recv.at[p]

    def x_copy(a, p):
        return remote(refs[a].at[:, lanes_of(1 - x, p)], landing(a, p).at[rows_of(x), :], x_send, x_sem(a, p), sp=side)

    def x_own(a, p):
        return pltpu.make_async_copy(refs[a].at[:, lanes_of(x, p)], landing(a, p).at[rows_of(x), :], x_sem(a, p))

    def landed(ref, sem):
        remote(ref, ref, x_send, sem, sp=side).wait_recv()

    def left(ref, sem):
        remote(ref, ref, sem, w_recv.at[0], sp=side).wait_send()

    def queries_here(p):
        landed(qx.at[p], q_recv.at[p])

    def keys_here(p):
        landed(kvx.at[p], kv_recv.at[p])

    g_copy = remote(g_ref.at[1 - x], gb.at[me], g_send.at[0], g_recv.at[0], sp=side)
    g_own = pltpu.make_async_copy(g_ref.at[x], gb.at[me], g_recv.at[1])

    def z_own(a, slot, target, p):
        return remote(refs[a].at[:, lanes_of(x, p)], zin.at[p, slot, rows_of(x), :],
                      z_send, z_recv.at[p], sp=target * 2 + x)

    def z_side(a, slot, target, p):
        return remote(landing(a, p).at[rows_of(1 - x), :], zin.at[p, slot, rows_of(1 - x), :],
                      z_send, z_recv.at[p], sp=target * 2 + x)

    up = ((1, 0, 1), (2, 1, 1))
    down_two = ((0, 2, 1),)
    down_three = ((0, 3, 1), (0, 2, 2))

    def sided(j, other):
        which = 1 - x if other else x
        return pairs // 2 + j + quarter * which

    def neighboured(j, other):
        which = 1 - odd if other else odd
        return quarter + j + step_z * which

    def w_of(r, q):
        return wall.at[r, :, q]

    def y_pair(u):
        return sided(u, False) if u < quarter else u - quarter

    def y_copy(u):
        return remote(w_ref.at[:, y_pair(u)], w_of(me_dp, y_pair(u)), w_send, y_recv.at[u], dp=across)

    def y_half(j, h):
        q = neighboured(j, False)
        return remote(w_ref.at[h, q], wall.at[me_dp, h, q], w_send, yh_recv.at[j, h], dp=across)

    def y_last(other=False):
        q = sided(quarter - 1, True)
        return remote(w_ref.at[1, q], wall.at[me_dp, 1, q], w_send, yh_recv.at[step_z, 0], dp=across)

    def side_copy(j, other=False):
        q = sided(j, other)
        ref = wall.at[across, 0, q] if j == quarter - 1 else w_of(across, q)
        return remote(ref, ref, w_send, wx_recv.at[j], sp=side)

    def near_copy(j, h, other=False):
        q = neighboured(j, other)
        return remote(wall.at[across, h, q], wall.at[across, h, q], w_send, wz_recv.at[j, h],
                      sp=other_z * 2 + x)

    def forward(q):
        return remote(w_of(across, q), w_of(across, q), w_send, w_recv.at[q], dp=partner)

    def p_copy(q):
        return remote(w_ref.at[:, q], w_of(me_dp, q), w_send, w_recv.at[q], dp=partner)

    def w_own(q):
        return pltpu.make_async_copy(w_ref.at[:, q], w_of(me_dp, q), w_recv.at[q])

    ahead = min(2, pairs)

    def lead(makers):
        for p in range(ahead):
            for make in makers:
                z_own(*make, p).start()

    def gates_out():
        g_copy.start()
        g_own.start()

    @pl.when(z == 0)
    def _():
        for p in range(pairs):
            for a in (1, 2):
                x_copy(a, p).start()
            if p == 0:
                gates_out()
                lead(up)
        for p in range(pairs):
            x_copy(0, p).start()

    @pl.when(z == 1)
    def _():
        for p in range(pairs):
            for a in (1, 2, 0):
                x_copy(a, p).start()
            if p == 0:
                gates_out()

    @pl.when(z >= 2)
    def _():
        for p in range(pairs):
            x_copy(0, p).start()
            if p == 0:
                @pl.when(z == 2)
                def _():
                    lead(down_two)

                @pl.when(z == 3)
                def _():
                    lead(down_three)
        gates_out()
        for p in range(pairs):
            for a in (1, 2):
                x_copy(a, p).start()

    for j in range(step_z):
        for h in range(2):
            y_half(j, h).start()
    for u in range(units):
        y_copy(u).start()
    y_last().start()
    for p in range(pairs):
        for a in range(3):
            x_own(a, p).start()

    def pass_on(u):
        y_copy(u).wait_recv()
        if u < quarter:
            side_copy(u).start()
        forward(y_pair(u)).start()

    def pass_loan(j):
        side_copy(j, True).wait_recv()
        if j == quarter - 1:
            y_last().wait_recv()
        forward(sided(j, True)).start()

    def near_here(h):
        for j in range(step_z):
            y_half(j, h).wait_recv()
            if h == 1:
                forward(neighboured(j, False)).start()

    def near_lend(h):
        for j in range(step_z):
            near_copy(j, h).start()

    def near_loan():
        for j in range(step_z):
            for h in range(2):
                near_copy(j, h, True).wait_recv()
            forward(neighboured(j, True)).start()

    def share_weights(p):
        p_copy(p).start()
        w_own(p).start()

    def part_copies(k, slot, p, target):
        return (
            remote(part_o.at[k, p], got_o.at[p, slot], po_send, po_recv.at[p], sp=target * 2 + x),
            remote(part_l.at[k, p], got_l.at[p, slot], pl_send, pl_recv.at[p], sp=target * 2 + x),
        )

    def o_copy(p):
        return remote(ob.at[p, rows_of(1 - x), :], att.at[p, :, half_of(x)], o_send, o_recv.at[p], sp=side)

    def gates_of(block, p):
        return jnp.concatenate([gb[2 * block, p], gb[2 * block + 1, p]], axis=1)

    def finish(p, value):
        ob[p] = value.astype(jnp.bfloat16)
        o_copy(p).start()
        att[p, :, half_of(x)] = ob[p, rows_of(x), :]

    def share(p, k, slot, target, value, lse):
        part_o[k, p] = value.astype(jnp.bfloat16)
        turned = jnp.transpose(lse)
        part_l[k, p] = jnp.concatenate([turned[0:1], turned[HEAD_DIM:HEAD_DIM + 1]], axis=0)
        for copy in part_copies(k, slot, p, target):
            copy.start()

    def join(p, slots):
        outs, sums = [held_o[p]], [held_l[p]]
        landed(got_o.at[p] if len(slots) == 2 else got_o.at[p, 0], po_recv.at[p])
        landed(got_l.at[p] if len(slots) == 2 else got_l.at[p, 0], pl_recv.at[p])
        for slot in slots:
            outs.append(got_o[p, slot].astype(jnp.float32))
            lse = got_l[p, slot]
            sums.append(jnp.transpose(jnp.concatenate(
                [jnp.broadcast_to(lse[h:h + 1], (HEAD_DIM, 2 * L)) for h in range(2)], axis=0)))
        peak = functools.reduce(jnp.maximum, sums)
        scale = [jnp.exp(s - peak) for s in sums]
        finish(p, sum(o * s for o, s in zip(outs, scale)) / sum(scale))

    def each(body, begin=0, end=None):
        def step(p, carry):
            body(p)
            return carry
        lax.fori_loop(begin, pairs if end is None else end, step, 0)

    def gates_here():
        g_own.wait()
        g_copy.wait_recv()

    def gates_up(target):
        return remote(gb.at[pl.ds(0, 2)], gb.at[pl.ds(0, 2)], g_send.at[1], g_recv.at[2], sp=target * 2 + x)

    def passing(p, table):
        for at, calls in table.items():
            @pl.when(p == at)
            def _(calls=calls):
                for call in calls:
                    call()

    def on(u):
        return lambda: pass_on(u)

    def near_all():
        near_here(0)
        near_here(1)

    def near_lend_all():
        near_lend(0)
        near_lend(1)

    def push(p, makers):
        for make in makers:
            z_side(*make, p).start()
        @pl.when(p + ahead < pairs)
        def _():
            for make in makers:
                z_own(*make, p + ahead).start()

    @pl.when(z == 0)
    def _():
        def pushes(p):
            keys_here(p)
            push(p, up)
            @pl.when(p == 0)
            def _():
                gates_here()
                gates_up(1).start()
        each(pushes)
        def work(p):
            queries_here(p)
            finish(p, attend_rows(qx[p], [(kvx[p, 0], kvx[p, 1], gates_of(0, p))], True)[0])
            share_weights(p)
            passing(p, {0: [near_all], 3: [on(0)], 7: [on(1)]})
        each(work)
        near_lend_all()
        near_loan()
        pass_on(2)

    @pl.when(z == 1)
    def _():
        gates_here()
        gates_up(0).wait_recv()
        def work(p):
            keys_here(p)
            landed(zin.at[p], z_recv.at[p])
            lower = (zin[p, 0], zin[p, 1], gates_of(0, p))
            own = (kvx[p, 0], kvx[p, 1], gates_of(1, p))
            for k in (1, 0):
                share(p, k, 0, 2 + k, *attend_rows(zin[p, 2 + k], [lower, own], False))
            queries_here(p)
            finish(p, attend_rows(qx[p], [lower, own], True)[0])
            share_weights(p)
            passing(p, {0: [near_all, near_lend_all], 1: [on(0)], 3: [on(1)], 5: [on(2)]})
        each(work)

    @pl.when(z == 2)
    def _():
        def pushes(p):
            queries_here(p)
            push(p, down_two)
            passing(p, {2: [lambda: near_here(0), lambda: near_lend(0)], 6: [lambda: near_here(1), lambda: near_lend(1)]})
        each(pushes)
        gates_here()
        lag = min(2, pairs)
        def work(p):
            keys_here(p)
            own = (kvx[p, 0], kvx[p, 1], gates_of(2, p))
            landed(zin.at[p, 2], z_recv.at[p])
            share(p, 1, 1, 3, *attend_rows(zin[p, 2], [own], False))
            held_o[p], held_l[p] = attend_rows(qx[p], [own], True)
            @pl.when(p >= lag)
            def _():
                join(p - lag, (0,))
            share_weights(p)
            passing(p, {2: [on(0)], 4: [on(1)], 6: [on(2)]})
        each(work)
        each(lambda p: join(p, (0,)), pairs - lag)

    @pl.when(z == 3)
    def _():
        def pushes(p):
            queries_here(p)
            push(p, down_three)
        each(pushes)
        gates_here()
        def work(p):
            keys_here(p)
            held_o[p], held_l[p] = attend_rows(qx[p], [(kvx[p, 0], kvx[p, 1], gates_of(3, p))], True)
            share_weights(p)
            passing(p, {0: [near_all, near_lend_all], 2: [near_loan], 4: [on(0)], 7: [on(1)]})
        each(work)
        def last(p):
            join(p, (0, 1))
            passing(p, {4: [on(2)]})
        each(last)

    for u in range(3, units):
        pass_on(u)
    pass_loan(0)

    @pl.when((z == 1) | (z == 2))
    def _():
        near_loan()

    for j in range(1, quarter):
        pass_loan(j)

    for at, q in enumerate(range(pairs)):
        landed(wall.at[pl.ds(0, 3), :, q], w_recv.at[q])
        o_copy(q).wait_recv()
        lhs = att[q]
        for r in range(ndp):
            columns = slice(r * w_cols, (r + 1) * w_cols)
            part = jnp.dot(lhs, wall[r, :, q].reshape(2 * LANES, w_cols), preferred_element_type=jnp.float32)
            if at > 0:
                part = acc[:, columns] + part
            if at < pairs - 1:
                acc[:, columns] = part
            else:
                o_ref[:, columns] = part.astype(o_ref.dtype)

    g_copy.wait_send()

    @pl.when(z == 0)
    def _():
        left(wall.at[0, 0], z_send)
        gates_up(1).wait_send()

    @pl.when(z == 1)
    def _():
        left(part_o, po_send)
        left(part_l, pl_send)

    @pl.when(z == 2)
    def _():
        left(wall.at[0, 0, pl.ds(0, pairs // 2)], z_send)
        left(part_o.at[1], po_send)
        left(part_l.at[1], pl_send)

    @pl.when(z == 3)
    def _():
        left(wall.at[0, 0], z_send)

    left(ob.at[:, pl.ds(0, L), :], o_send)
    left(wall.at[0, 0, pl.ds(0, 3 * pairs // 4)], x_send)
    left(wall.at[pl.ds(0, 3)], w_send)


def fused(n, ndp, queries, keys, values, gate_totals, w_out):
    L, model = queries.shape[1], queries.shape[2]
    heads = gate_totals.shape[2] // 2
    pairs = heads * HEAD_DIM // LANES
    gates = jnp.transpose(gate_totals[0]).reshape(2, pairs, 2, L)
    w_cols = w_out.shape[1]
    weights = w_out.reshape(2, pairs, LANES, w_cols)
    bf16, f32 = jnp.bfloat16, jnp.float32
    dma = pltpu.SemaphoreType.DMA
    block = (pairs, 2 * L, LANES)
    quarter = pairs // 4
    units, step_z = 2 * quarter, quarter // 2
    out = pl.pallas_call(
        functools.partial(kernel, n, ndp),
        out_shape=jax.ShapeDtypeStruct((L, w_cols * ndp), bf16),
        in_specs=[pl.BlockSpec(memory_space=pltpu.HBM)] * 5,
        out_specs=pl.BlockSpec(memory_space=pltpu.VMEM),
        scratch_shapes=[
            pltpu.VMEM(block, bf16),
            pltpu.VMEM((pairs, 2) + block[1:], bf16),
            pltpu.VMEM((pairs, 4) + block[1:], bf16),
            pltpu.VMEM((n, pairs, 2, L), f32),
            pltpu.VMEM(block, bf16),
            pltpu.VMEM(block, f32),
            pltpu.VMEM(block, f32),
            pltpu.VMEM((2,) + block, bf16),
            pltpu.VMEM((2, pairs, 2, 2 * L), f32),
            pltpu.VMEM((pairs, 2) + block[1:], bf16),
            pltpu.VMEM((pairs, 2, 2, 2 * L), f32),
            pltpu.VMEM((pairs, L, 2 * LANES), bf16),
            pltpu.VMEM((ndp, 2, pairs, LANES, w_cols), bf16),
            pltpu.VMEM((L, ndp * w_cols), f32),
            dma((pairs,)), dma((pairs,)), dma, dma((2,)), dma((3,)), dma, dma((pairs,)),
            dma, dma((pairs,)), dma, dma((pairs,)),
            dma, dma((pairs,)), dma((units,)), dma((step_z + 1, 2)), dma((quarter,)), dma((step_z, 2)),
            dma((pairs,)), dma,
        ],
        compiler_params=pltpu.CompilerParams(
            collective_id=0, has_side_effects=True, vmem_limit_bytes=48 * 2**20),
        name="fused_attention",
    )(*[pltpu.with_memory_space_constraint(t, pltpu.HBM) for t in (queries[0], keys[0], values[0], gates, weights)])
    return out[None]


def solution(mesh):
    n, ndp = mesh.shape["sp"], mesh.shape["dp"]

    def local(queries, keys, values, gate_totals, w_out):
        fits = n == 8 and ndp == 4 and queries.shape[1] % LANES == 0 and queries.shape[2] == 2 * n * LANES
        if fits:
            return fused(n, ndp, queries, keys, values, gate_totals, w_out)
        return general(queries, keys, values, gate_totals, w_out)

    placed = (P("dp", "sp", None),) * 4 + (P(None, "dp"),)
    return jax.shard_map(
        local, mesh=mesh, in_specs=placed, out_specs=P("dp", "sp", None), check_vma=False)
```

time: 47.6 us -> 42.1 us (0.88)
  the two profiles are of different devices: /device:TPU:11 before, /device:TPU:24 now
where the time goes in v2:
time: 42.1 us; the launch traced here: 42 us
  Pallas kernels  41.2 us (98%)
  local copies, waits for them, and re-layouts  0.8 us (2%)
    pallas_call x1, Pallas kernels, fused(): pl.pallas_call(functools.partial(kernel, n, ndp), out_shape=jax.ShapeDtyp...  41.2 us

profile of v2, /device:TPU:24, one launch (start us, length us, event | category | flops | bytes accessed | tf_op | source)
XLA Modules:
  0.0 42.0 jit_solution(6741176038925964067)
XLA Ops:
  0.0 41.2 %fused_attention.1 = bf16[128,2048]{1,0:T(8,128)(2,1)S(1)} custom-call(bf16[128,2048]{1,0:T(8,128)(2,1)} %bitcast.12, bf16[128,2048]{1,0:T(8,128)(2,1)} %bitcast.13, bf16[128,2048]{1,0:T(8,128)(2,1)} %bitcast.14, f32[2,8,2,128]{3,2,1,0:T(2,128)} %bitcast.15, bf16[2,8,128,512]{3,2,1,0:T(8,128)(2,1)} %bitcast.11), custom_call_target="tpu_custom_call" | custom-call | tf_op jit(solution)/shard_map/fused_attention/pallas_call | solution.py:536
  41.2 0.8 %copy.7 = bf16[1,128,2048]{2,1,0:T(8,128)(2,1)} copy(bf16[1,128,2048]{2,1,0:T(8,128)(2,1)S(1)} %bitcast.10) | data formatting | bytes 1048576

commit v3 on v2

--- a/solution.py
+++ b/solution.py
@@ -9,7 +9,7 @@
 
 HEAD_DIM = 64
 LANES = 128
-W_CHUNKS = 16
+LOG2E = 1.4426950408889634
 MESH = pl.DeviceIdType.MESH
 
 
@@ -60,38 +60,46 @@
     return mixed.astype(jnp.bfloat16)[None]
 
 
-def attend_rows(queries, parts, diagonal):
-    rows = queries.shape[0]
-    scaled = queries * jnp.bfloat16(HEAD_DIM ** -0.5)
-    lane = lax.broadcasted_iota(jnp.int32, (rows, LANES), 1)
-    outs, sums = [], []
-    for h in range(2):
-        mine = (lane < HEAD_DIM) if h == 0 else (lane >= HEAD_DIM)
-        scores = []
-        for at, (keys, _, gates) in enumerate(parts):
-            head_keys = jnp.where(mine, keys, jnp.zeros_like(keys))
-            score = lax.dot_general(
-                scaled, head_keys, (((1,), (1,)), ((), ())), preferred_element_type=jnp.float32)
-            score = score - gates[h:h + 1, :]
-            if diagonal and at == len(parts) - 1:
-                causal = lax.broadcasted_iota(jnp.int32, score.shape, 1) <= lax.broadcasted_iota(
-                    jnp.int32, score.shape, 0)
-                score = jnp.where(causal, score, -jnp.inf)
-            scores.append(score)
-        peak = functools.reduce(jnp.maximum, [jnp.max(x, axis=1, keepdims=True) for x in scores])
-        expo = [jnp.exp(x - peak) for x in scores]
-        total = sum(jnp.sum(x, axis=1, keepdims=True) for x in expo)
-        out = sum(
-            jnp.dot(x.astype(jnp.bfloat16), part[1], preferred_element_type=jnp.float32)
-            for x, part in zip(expo, parts))
-        outs.append(out / total)
-        sums.append(peak + jnp.log(total))
-    first = lane < HEAD_DIM
-    return jnp.where(first, outs[0], outs[1]), jnp.where(first, sums[0], sums[1])
+def attend_rows(tasks, parts):
+    def of_head(h, array, other):
+        lane = lax.broadcasted_iota(jnp.int32, array.shape, 1)
+        return jnp.where((lane < HEAD_DIM) if h == 0 else (lane >= HEAD_DIM), array, jnp.full_like(array, other))
+
+    chains = [(i, h) for i in range(len(tasks)) for h in range(2)]
+    scaled = [queries * jnp.bfloat16(HEAD_DIM ** -0.5) for queries, _ in tasks]
+    head_keys = [[of_head(h, part[0], 0) for part in parts] for h in range(2)]
+    head_values = [[of_head(h, part[1], 1) for part in parts] for h in range(2)]
+    gates = [part[2] * LOG2E for part in parts]
+    scores, peaks, weights, sums = {}, {}, {}, {}
+    for i, h in chains:
+        scores[i, h] = [
+            lax.dot_general(scaled[i], keys, (((1,), (1,)), ((), ())), preferred_element_type=jnp.float32)
+            for keys in head_keys[h]]
+    for i, h in chains:
+        rows = [score * LOG2E - gate[h:h + 1, :] for score, gate in zip(scores[i, h], gates)]
+        if tasks[i][1]:
+            shape = rows[-1].shape
+            causal = lax.broadcasted_iota(jnp.int32, shape, 1) <= lax.broadcasted_iota(jnp.int32, shape, 0)
+            rows[-1] = jnp.where(causal, rows[-1], -jnp.inf)
+        scores[i, h] = rows
+        peaks[i, h] = functools.reduce(jnp.maximum, [jnp.max(x, axis=1, keepdims=True) for x in rows])
+    for i, h in chains:
+        weights[i, h] = [jnp.exp2(x - peaks[i, h]).astype(jnp.bfloat16) for x in scores[i, h]]
+    for i, h in chains:
+        sums[i, h] = sum(
+            jnp.dot(x, values, preferred_element_type=jnp.float32)
+            for x, values in zip(weights[i, h], head_values[h]))
+    results = []
+    for i in range(len(tasks)):
+        first = lax.broadcasted_iota(jnp.int32, sums[i, 0].shape, 1) < HEAD_DIM
+        out = jnp.where(first, sums[i, 0], sums[i, 1])
+        total = pltpu.roll(jnp.where(first, sums[i, 1], sums[i, 0]), HEAD_DIM, 1)
+        results.append((out / total, jnp.where(first, peaks[i, 0], peaks[i, 1]) + jnp.log2(total)))
+    return results
 
 
 def kernel(n, ndp, q_ref, k_ref, v_ref, g_ref, w_ref, o_ref,
-           qx, kvx, zin, gb, ob, held_o, held_l, part_o, part_l, got_o, got_l, att, wall, acc,
+           qx, kvx, zin, gb, ob, held_o, held_l, near_o, near_l, part_o, part_l, got_o, got_l, att, wall, acc,
            q_recv, kv_recv, x_send, g_send, g_recv, z_send, z_recv, po_send, po_recv, pl_send, pl_recv,
            o_send, o_recv, y_recv, yh_recv, wx_recv, wz_recv, w_recv, w_send):
     me = lax.axis_index("sp")
@@ -180,7 +188,6 @@
 
     up = ((1, 0, 1), (2, 1, 1))
     down_two = ((0, 2, 1),)
-    down_three = ((0, 3, 1), (0, 2, 2))
 
     def sided(j, other):
         which = 1 - x if other else x
@@ -226,7 +233,8 @@
     def w_own(q):
         return pltpu.make_async_copy(w_ref.at[:, q], w_of(me_dp, q), w_recv.at[q])
 
-    ahead = min(2, pairs)
+    direct = pairs - 2
+    ahead = min(3, pairs)
 
     def lead(makers):
         for p in range(ahead):
@@ -256,18 +264,31 @@
             if p == 0:
                 gates_out()
 
-    @pl.when(z >= 2)
-    def _():
-        for p in range(pairs):
+    @pl.when(z == 2)
+    def _():
+        for p in range(ahead):
             x_copy(0, p).start()
             if p == 0:
-                @pl.when(z == 2)
-                def _():
-                    lead(down_two)
-
-                @pl.when(z == 3)
-                def _():
-                    lead(down_three)
+                lead(down_two)
+            if p + direct < pairs:
+                x_copy(0, p + direct).start()
+        gates_out()
+        for i in range(pairs):
+            for a in (1, 2):
+                x_copy(a, (i + direct) % pairs).start()
+            if i + ahead < direct:
+                x_copy(0, i + ahead).start()
+
+    @pl.when(z == 3)
+    def _():
+        for p in range(direct):
+            x_copy(0, p).start()
+            if p + direct < pairs:
+                x_copy(0, p + direct).start()
+            if p == 0:
+                for i in range(ahead):
+                    z_own(0, 3, 1, i).start()
+                    z_own(0, 2, 2, (i + direct) % pairs).start()
         gates_out()
         for p in range(pairs):
             for a in (1, 2):
@@ -332,25 +353,58 @@
         o_copy(p).start()
         att[p, :, half_of(x)] = ob[p, rows_of(x), :]
 
+    def send_part(p, k, slot, target):
+        for copy in part_copies(k, slot, p, target):
+            copy.start()
+
     def share(p, k, slot, target, value, lse):
+        store_part(p, k, value, lse)
+        send_part(p, k, slot, target)
+
+    def store_part(p, k, value, lse):
         part_o[k, p] = value.astype(jnp.bfloat16)
         turned = jnp.transpose(lse)
         part_l[k, p] = jnp.concatenate([turned[0:1], turned[HEAD_DIM:HEAD_DIM + 1]], axis=0)
-        for copy in part_copies(k, slot, p, target):
-            copy.start()
-
-    def join(p, slots):
-        outs, sums = [held_o[p]], [held_l[p]]
-        landed(got_o.at[p] if len(slots) == 2 else got_o.at[p, 0], po_recv.at[p])
-        landed(got_l.at[p] if len(slots) == 2 else got_l.at[p, 0], pl_recv.at[p])
+
+    def merged(p, o_ref, l_ref, slots):
+        outs, sums = [o_ref[p]], [l_ref[p]]
         for slot in slots:
             outs.append(got_o[p, slot].astype(jnp.float32))
             lse = got_l[p, slot]
             sums.append(jnp.transpose(jnp.concatenate(
                 [jnp.broadcast_to(lse[h:h + 1], (HEAD_DIM, 2 * L)) for h in range(2)], axis=0)))
         peak = functools.reduce(jnp.maximum, sums)
-        scale = [jnp.exp(s - peak) for s in sums]
-        finish(p, sum(o * s for o, s in zip(outs, scale)) / sum(scale))
+        scale = [jnp.exp2(s - peak) for s in sums]
+        total = sum(scale)
+        return sum(o * s for o, s in zip(outs, scale)) / total, peak + jnp.log2(total)
+
+    def parts_here(p, slots):
+        landed(got_o.at[p] if len(slots) == 2 else got_o.at[p, slots[0]], po_recv.at[p])
+        landed(got_l.at[p] if len(slots) == 2 else got_l.at[p, slots[0]], pl_recv.at[p])
+
+    def join(p, slots):
+        parts_here(p, slots)
+        finish(p, merged(p, held_o, held_l, slots)[0])
+
+    def join_two(p):
+        @pl.when(p < direct)
+        def _():
+            parts_here(p, (0, 1))
+            share(p, 1, 1, 3, *merged(p, near_o, near_l, (1,)))
+            finish(p, merged(p, held_o, held_l, (0,))[0])
+
+        @pl.when(p >= direct)
+        def _():
+            join(p, (0,))
+
+    def join_three(p):
+        @pl.when(p < direct)
+        def _():
+            join(p, (1,))
+
+        @pl.when(p >= direct)
+        def _():
+            join(p, (0, 1))
 
     def each(body, begin=0, end=None):
         def step(p, carry):
@@ -403,7 +457,7 @@
         each(pushes)
         def work(p):
             queries_here(p)
-            finish(p, attend_rows(qx[p], [(kvx[p, 0], kvx[p, 1], gates_of(0, p))], True)[0])
+            finish(p, attend_rows([(qx[p], True)], [(kvx[p, 0], kvx[p, 1], gates_of(0, p))])[0][0])
             share_weights(p)
             passing(p, {0: [near_all], 3: [on(0)], 7: [on(1)]})
         each(work)
@@ -420,67 +474,112 @@
             landed(zin.at[p], z_recv.at[p])
             lower = (zin[p, 0], zin[p, 1], gates_of(0, p))
             own = (kvx[p, 0], kvx[p, 1], gates_of(1, p))
-            for k in (1, 0):
-                share(p, k, 0, 2 + k, *attend_rows(zin[p, 2 + k], [lower, own], False))
             queries_here(p)
-            finish(p, attend_rows(qx[p], [lower, own], True)[0])
+            three, two, one = attend_rows([(zin[p, 3], False), (zin[p, 2], False), (qx[p], True)], [lower, own])
+            store_part(p, 1, *three)
+            @pl.when(p < direct)
+            def _():
+                send_part(p, 1, 1, 2)
+
+            @pl.when(p >= direct)
+            def _():
+                send_part(p, 1, 0, 3)
+            share(p, 0, 0, 2, *two)
+            finish(p, one[0])
             share_weights(p)
-            passing(p, {0: [near_all, near_lend_all], 1: [on(0)], 3: [on(1)], 5: [on(2)]})
+            passing(p, {0: [near_all, near_lend_all], 2: [on(0)], 4: [on(1)], 6: [on(2)]})
         each(work)
 
     @pl.when(z == 2)
     def _():
-        def pushes(p):
+        for p in range(ahead):
             queries_here(p)
             push(p, down_two)
-            passing(p, {2: [lambda: near_here(0), lambda: near_lend(0)], 6: [lambda: near_here(1), lambda: near_lend(1)]})
-        each(pushes)
+            if p + direct < pairs:
+                queries_here(p + direct)
+        near_here(0)
+        near_lend(0)
         gates_here()
-        lag = min(2, pairs)
-        def work(p):
+        lag = pairs - direct
+        def work(i):
+            p = lax.rem(i + direct, pairs)
             keys_here(p)
             own = (kvx[p, 0], kvx[p, 1], gates_of(2, p))
             landed(zin.at[p, 2], z_recv.at[p])
-            share(p, 1, 1, 3, *attend_rows(zin[p, 2], [own], False))
-            held_o[p], held_l[p] = attend_rows(qx[p], [own], True)
-            @pl.when(p >= lag)
+            three, (held_o[p], held_l[p]) = attend_rows([(zin[p, 2], False), (qx[p], True)], [own])
+            near_o[p], near_l[p] = three
+            @pl.when(p >= direct)
             def _():
-                join(p - lag, (0,))
+                share(p, 1, 1, 3, near_o[p], near_l[p])
+            @pl.when(i + ahead < pairs)
+            def _():
+                @pl.when(i + ahead < direct)
+                def _():
+                    queries_here(i + ahead)
+                push(i + ahead, down_two)
+            passing(i, {0: [lambda: near_here(1), lambda: near_lend(1)], 3: [on(0)], 5: [on(1)]})
+            @pl.when(i >= lag)
+            def _():
+                join_two(i - lag)
             share_weights(p)
-            passing(p, {2: [on(0)], 4: [on(1)], 6: [on(2)]})
+            passing(i, {pairs - 1: [on(2)]})
         each(work)
-        each(lambda p: join(p, (0,)), pairs - lag)
+        def last(p):
+            join_two(p)
+            passing(p, {pairs - 2: [lambda: pass_loan(0), on(3)]})
+        each(last, direct)
 
     @pl.when(z == 3)
     def _():
-        def pushes(p):
-            queries_here(p)
-            push(p, down_three)
-        each(pushes)
+        for i in range(pairs):
+            if i < direct:
+                queries_here(i)
+            if i + direct < pairs:
+                queries_here(i + direct)
+            near = (i + direct) % pairs
+            z_side(0, 3, 1, i).start()
+            z_side(0, 2, 2, near).start()
+            if i + ahead < pairs:
+                z_own(0, 3, 1, i + ahead).start()
+                z_own(0, 2, 2, (near + ahead) % pairs).start()
         gates_here()
         def work(p):
             keys_here(p)
-            held_o[p], held_l[p] = attend_rows(qx[p], [(kvx[p, 0], kvx[p, 1], gates_of(3, p))], True)
+            held_o[p], held_l[p] = attend_rows([(qx[p], True)], [(kvx[p, 0], kvx[p, 1], gates_of(3, p))])[0]
             share_weights(p)
-            passing(p, {0: [near_all, near_lend_all], 2: [near_loan], 4: [on(0)], 7: [on(1)]})
+            passing(p, {0: [near_all, near_lend_all], 4: [on(0)], 7: [near_loan, on(1)]})
         each(work)
         def last(p):
-            join(p, (0, 1))
-            passing(p, {4: [on(2)]})
+            join_three(p)
+            passing(p, {3: [on(2)], 4: [lambda: pass_loan(0)], 6: [on(3)]})
         each(last)
 
-    for u in range(3, units):
-        pass_on(u)
-    pass_loan(0)
-
-    @pl.when((z == 1) | (z == 2))
-    def _():
+    @pl.when(z == 0)
+    def _():
+        pass_loan(0)
+        pass_on(3)
+
+    @pl.when(z == 1)
+    def _():
+        pass_loan(0)
         near_loan()
-
-    for j in range(1, quarter):
-        pass_loan(j)
-
-    for at, q in enumerate(range(pairs)):
+        pass_on(3)
+
+    @pl.when(z == 2)
+    def _():
+        near_loan()
+
+    @pl.when(z >= 2)
+    def _():
+        pass_loan(1)
+
+    early = list(range(pairs - 3)) + [pairs - 3 + x]
+    steps = early + [pairs - 2 - x, pairs - 1]
+    for at, q in enumerate(steps):
+        if at == len(early):
+            @pl.when(z < 2)
+            def _():
+                pass_loan(1)
         landed(wall.at[pl.ds(0, 3), :, q], w_recv.at[q])
         o_copy(q).wait_recv()
         lhs = att[q]
@@ -544,8 +643,7 @@
             pltpu.VMEM((pairs, 4) + block[1:], bf16),
             pltpu.VMEM((n, pairs, 2, L), f32),
             pltpu.VMEM(block, bf16),
-            pltpu.VMEM(block, f32),
-            pltpu.VMEM(block, f32),
+            *[pltpu.VMEM(block, f32)] * 4,
             pltpu.VMEM((2,) + block, bf16),
             pltpu.VMEM((2, pairs, 2, 2 * L), f32),
             pltpu.VMEM((pairs, 2) + block[1:], bf16),

time: 42.1 us -> 41 us (0.974)
  Pallas kernels: 41.2 us -> 40 us
    pallas_call x1, Pallas kernels: 41.2 us -> 40 us  [fused(): pl.pallas_call(functools.partial(kernel, n, ndp), out_shape=jax.ShapeDtyp...]
where the time goes in v3:
time: 41 us; the launch traced here: 40.8 us
  Pallas kernels  40 us (98%)
  local copies, waits for them, and re-layouts  0.8 us (2%)
    pallas_call x1, Pallas kernels, fused(): pl.pallas_call(functools.partial(kernel, n, ndp), out_shape=jax.ShapeDtyp...  40 us

profile of v3, /device:TPU:24, one launch (start us, length us, event | category | flops | bytes accessed | tf_op | source)
XLA Modules:
  0.0 40.8 jit_solution(13600058744123640272)
XLA Ops:
  0.0 40.0 %fused_attention.1 = bf16[128,2048]{1,0:T(8,128)(2,1)S(1)} custom-call(bf16[128,2048]{1,0:T(8,128)(2,1)} %bitcast.12, bf16[128,2048]{1,0:T(8,128)(2,1)} %bitcast.13, bf16[128,2048]{1,0:T(8,128)(2,1)} %bitcast.14, f32[2,8,2,128]{3,2,1,0:T(2,128)} %bitcast.15, bf16[2,8,128,512]{3,2,1,0:T(8,128)(2,1)} %bitcast.11), custom_call_target="tpu_custom_call" | custom-call | tf_op jit(solution)/shard_map/fused_attention/pallas_call | solution.py:635
  40.0 0.8 %copy.7 = bf16[1,128,2048]{2,1,0:T(8,128)(2,1)} copy(bf16[1,128,2048]{2,1,0:T(8,128)(2,1)S(1)} %bitcast.10) | data formatting | bytes 1048576

commit v4 on v3

--- a/solution.py
+++ b/solution.py
@@ -99,9 +99,9 @@
 
 
 def kernel(n, ndp, q_ref, k_ref, v_ref, g_ref, w_ref, o_ref,
-           qx, kvx, zin, gb, ob, held_o, held_l, near_o, near_l, part_o, part_l, got_o, got_l, att, wall, acc,
+           qx, kvx, zin, gb, ob, held_o, held_l, near_o, near_l, part_o, part_l, got_o, got_l, tail_o, tail_l, att, wall, acc,
            q_recv, kv_recv, x_send, g_send, g_recv, z_send, z_recv, po_send, po_recv, pl_send, pl_recv,
-           o_send, o_recv, y_recv, yh_recv, wx_recv, wz_recv, w_recv, w_send):
+           o_send, o_recv, t_recv, y_recv, yh_recv, wx_recv, wz_recv, w_recv, w_send):
     me = lax.axis_index("sp")
     x = lax.rem(me, 2)
     z = lax.div(me, 2)
@@ -233,7 +233,7 @@
     def w_own(q):
         return pltpu.make_async_copy(w_ref.at[:, q], w_of(me_dp, q), w_recv.at[q])
 
-    direct = pairs - 2
+    direct = pairs - 3
     ahead = min(3, pairs)
 
     def lead(makers):
@@ -247,22 +247,20 @@
 
     @pl.when(z == 0)
     def _():
+        gates_out()
+        lead(up)
         for p in range(pairs):
             for a in (1, 2):
                 x_copy(a, p).start()
-            if p == 0:
-                gates_out()
-                lead(up)
         for p in range(pairs):
             x_copy(0, p).start()
 
     @pl.when(z == 1)
     def _():
+        gates_out()
         for p in range(pairs):
             for a in (1, 2, 0):
                 x_copy(a, p).start()
-            if p == 0:
-                gates_out()
 
     @pl.when(z == 2)
     def _():
@@ -353,9 +351,58 @@
         o_copy(p).start()
         att[p, :, half_of(x)] = ob[p, rows_of(x), :]
 
+    final = pairs - 1
+
+    def tail_copies(k, slot, target, row, o_sem, l_sem):
+        return (
+            remote(part_o.at[k, final, rows_of(row), :], tail_o.at[slot, x], o_sem, t_recv.at[slot, 0],
+                   sp=target * 2 + row),
+            remote(part_l.at[k, final, :, rows_of(row)], tail_l.at[slot, x], l_sem, t_recv.at[slot, 1],
+                   sp=target * 2 + row),
+        )
+
     def send_part(p, k, slot, target):
-        for copy in part_copies(k, slot, p, target):
-            copy.start()
+        @pl.when(p < final)
+        def _():
+            for copy in part_copies(k, slot, p, target):
+                copy.start()
+
+        @pl.when(p == final)
+        def _():
+            for row in (1 - x, x):
+                for copy in tail_copies(k, slot, target, row, po_send, pl_send):
+                    copy.start()
+
+    def hold(p, value, lse):
+        @pl.when(p < final)
+        def _():
+            held_o[p], held_l[p] = value, lse
+
+        @pl.when(p == final)
+        def _():
+            store_part(final, 0, value, lse)
+            for copy in tail_copies(0, 2, z, 1 - x, o_send, g_send.at[1]):
+                copy.start()
+            tail_o[2, pl.ds(x, 1)] = part_o[0, final, rows_of(x), :][None]
+            tail_l[2, pl.ds(x, 1)] = part_l[0, final, :, rows_of(x)][None]
+
+    def join_tail(slots):
+        landed(tail_o.at[2, 1 - x], t_recv.at[2, 0])
+        landed(tail_l.at[2, 1 - x], t_recv.at[2, 1])
+        for slot in slots:
+            landed(tail_o.at[slot], t_recv.at[slot, 0])
+            landed(tail_l.at[slot], t_recv.at[slot, 1])
+        for h in range(2):
+            outs, sums = [], []
+            for slot in (2,) + slots:
+                outs.append(tail_o[slot, h].astype(jnp.float32))
+                lse = tail_l[slot, h]
+                sums.append(jnp.transpose(jnp.concatenate(
+                    [jnp.broadcast_to(lse[j:j + 1], (HEAD_DIM, L)) for j in range(2)], axis=0)))
+            peak = functools.reduce(jnp.maximum, sums)
+            scale = [jnp.exp2(s - peak) for s in sums]
+            value = sum(o * s for o, s in zip(outs, scale)) / sum(scale)
+            att[final, :, h * LANES:(h + 1) * LANES] = value.astype(jnp.bfloat16)
 
     def share(p, k, slot, target, value, lse):
         store_part(p, k, value, lse)
@@ -393,18 +440,26 @@
             share(p, 1, 1, 3, *merged(p, near_o, near_l, (1,)))
             finish(p, merged(p, held_o, held_l, (0,))[0])
 
-        @pl.when(p >= direct)
+        @pl.when((p >= direct) & (p < final))
         def _():
             join(p, (0,))
+
+        @pl.when(p == final)
+        def _():
+            join_tail((0,))
 
     def join_three(p):
         @pl.when(p < direct)
         def _():
             join(p, (1,))
 
-        @pl.when(p >= direct)
+        @pl.when((p >= direct) & (p < final))
         def _():
             join(p, (0, 1))
+
+        @pl.when(p == final)
+        def _():
+            join_tail((0, 1))
 
     def each(body, begin=0, end=None):
         def step(p, carry):
@@ -450,10 +505,8 @@
         def pushes(p):
             keys_here(p)
             push(p, up)
-            @pl.when(p == 0)
-            def _():
-                gates_here()
-                gates_up(1).start()
+        gates_here()
+        gates_up(1).start()
         each(pushes)
         def work(p):
             queries_here(p)
@@ -487,7 +540,7 @@
             share(p, 0, 0, 2, *two)
             finish(p, one[0])
             share_weights(p)
-            passing(p, {0: [near_all, near_lend_all], 2: [on(0)], 4: [on(1)], 6: [on(2)]})
+            passing(p, {0: [near_all, near_lend_all], 2: [on(0)], 4: [on(1)], 7: [on(2)]})
         each(work)
 
     @pl.when(z == 2)
@@ -506,8 +559,8 @@
             keys_here(p)
             own = (kvx[p, 0], kvx[p, 1], gates_of(2, p))
             landed(zin.at[p, 2], z_recv.at[p])
-            three, (held_o[p], held_l[p]) = attend_rows([(zin[p, 2], False), (qx[p], True)], [own])
-            near_o[p], near_l[p] = three
+            (near_o[p], near_l[p]), mine = attend_rows([(zin[p, 2], False), (qx[p], True)], [own])
+            hold(p, *mine)
             @pl.when(p >= direct)
             def _():
                 share(p, 1, 1, 3, near_o[p], near_l[p])
@@ -526,7 +579,7 @@
         each(work)
         def last(p):
             join_two(p)
-            passing(p, {pairs - 2: [lambda: pass_loan(0), on(3)]})
+            passing(p, {pairs - 2: [lambda: pass_loan(0), near_loan, on(3), lambda: pass_loan(1)]})
         each(last, direct)
 
     @pl.when(z == 3)
@@ -545,43 +598,36 @@
         gates_here()
         def work(p):
             keys_here(p)
-            held_o[p], held_l[p] = attend_rows([(qx[p], True)], [(kvx[p, 0], kvx[p, 1], gates_of(3, p))])[0]
+            hold(p, *attend_rows([(qx[p], True)], [(kvx[p, 0], kvx[p, 1], gates_of(3, p))])[0])
             share_weights(p)
             passing(p, {0: [near_all, near_lend_all], 4: [on(0)], 7: [near_loan, on(1)]})
         each(work)
         def last(p):
             join_three(p)
-            passing(p, {3: [on(2)], 4: [lambda: pass_loan(0)], 6: [on(3)]})
+            passing(p, {3: [on(2)], 4: [lambda: pass_loan(0)], 6: [on(3), lambda: pass_loan(1)]})
         each(last)
 
     @pl.when(z == 0)
     def _():
         pass_loan(0)
         pass_on(3)
+        pass_loan(1)
 
     @pl.when(z == 1)
     def _():
         pass_loan(0)
         near_loan()
         pass_on(3)
-
-    @pl.when(z == 2)
-    def _():
-        near_loan()
-
-    @pl.when(z >= 2)
-    def _():
         pass_loan(1)
 
-    early = list(range(pairs - 3)) + [pairs - 3 + x]
-    steps = early + [pairs - 2 - x, pairs - 1]
-    for at, q in enumerate(steps):
-        if at == len(early):
+    for at, q in enumerate(range(pairs)):
+        landed(wall.at[pl.ds(0, 3), :, q], w_recv.at[q])
+        if at < pairs - 1:
+            o_copy(q).wait_recv()
+        else:
             @pl.when(z < 2)
             def _():
-                pass_loan(1)
-        landed(wall.at[pl.ds(0, 3), :, q], w_recv.at[q])
-        o_copy(q).wait_recv()
+                o_copy(q).wait_recv()
         lhs = att[q]
         for r in range(ndp):
             columns = slice(r * w_cols, (r + 1) * w_cols)
@@ -614,6 +660,10 @@
     @pl.when(z == 3)
     def _():
         left(wall.at[0, 0], z_send)
+
+    @pl.when(z >= 2)
+    def _():
+        left(part_l.at[0, final, :, rows_of(1 - x)], g_send.at[1])
 
     left(ob.at[:, pl.ds(0, L), :], o_send)
     left(wall.at[0, 0, pl.ds(0, 3 * pairs // 4)], x_send)
@@ -648,12 +698,14 @@
             pltpu.VMEM((2, pairs, 2, 2 * L), f32),
             pltpu.VMEM((pairs, 2) + block[1:], bf16),
             pltpu.VMEM((pairs, 2, 2, 2 * L), f32),
+            pltpu.VMEM((3, 2, L, LANES), bf16),
+            pltpu.VMEM((3, 2, 2, L), f32),
             pltpu.VMEM((pairs, L, 2 * LANES), bf16),
             pltpu.VMEM((ndp, 2, pairs, LANES, w_cols), bf16),
             pltpu.VMEM((L, ndp * w_cols), f32),
             dma((pairs,)), dma((pairs,)), dma, dma((2,)), dma((3,)), dma, dma((pairs,)),
             dma, dma((pairs,)), dma, dma((pairs,)),
-            dma, dma((pairs,)), dma((units,)), dma((step_z + 1, 2)), dma((quarter,)), dma((step_z, 2)),
+            dma, dma((pairs,)), dma((3, 2)), dma((units,)), dma((step_z + 1, 2)), dma((quarter,)), dma((step_z, 2)),
             dma((pairs,)), dma,
         ],
         compiler_params=pltpu.CompilerParams(

time: 41 us -> 40 us (0.976)
  Pallas kernels: 40 us -> 38.7 us
    pallas_call x1, Pallas kernels: 40 us -> 38.7 us  [fused(): pl.pallas_call(functools.partial(kernel, n, ndp), out_shape=jax.ShapeDtyp...]
where the time goes in v4:
time: 40 us; the launch traced here: 39.5 us
  Pallas kernels  38.7 us (97%)
  local copies, waits for them, and re-layouts  0.8 us (2%)
    pallas_call x1, Pallas kernels, fused(): pl.pallas_call(functools.partial(kernel, n, ndp), out_shape=jax.ShapeDtyp...  38.7 us

profile of v4, /device:TPU:24, one launch (start us, length us, event | category | flops | bytes accessed | tf_op | source)
XLA Modules:
  0.0 39.5 jit_solution(7029625080992331565)
XLA Ops:
  0.0 38.7 %fused_attention.1 = bf16[128,2048]{1,0:T(8,128)(2,1)S(1)} custom-call(bf16[128,2048]{1,0:T(8,128)(2,1)} %bitcast.12, bf16[128,2048]{1,0:T(8,128)(2,1)} %bitcast.13, bf16[128,2048]{1,0:T(8,128)(2,1)} %bitcast.14, f32[2,8,2,128]{3,2,1,0:T(2,128)} %bitcast.15, bf16[2,8,128,512]{3,2,1,0:T(8,128)(2,1)} %bitcast.11), custom_call_target="tpu_custom_call" | custom-call | tf_op jit(solution)/shard_map/fused_attention/pallas_call | solution.py:685
  38.7 0.8 %copy.7 = bf16[1,128,2048]{2,1,0:T(8,128)(2,1)} copy(bf16[1,128,2048]{2,1,0:T(8,128)(2,1)S(1)} %bitcast.10) | data formatting | bytes 1048576

commit v5 on v4

--- a/solution.py
+++ b/solution.py
@@ -500,6 +500,32 @@
             for make in makers:
                 z_own(*make, p + ahead).start()
 
+    early = [q for q in range(pairs // 2) if q != 1]
+    late = [q for q in range(pairs) if q not in early]
+
+    def products(which):
+        for q in which:
+            landed(wall.at[pl.ds(0, 3), :, q], w_recv.at[q])
+            if q < final:
+                o_copy(q).wait_recv()
+            else:
+                @pl.when(z < 2)
+                def _():
+                    o_copy(q).wait_recv()
+            lhs = att[q]
+            for r in range(ndp):
+                columns = slice(r * w_cols, (r + 1) * w_cols)
+                part = jnp.dot(lhs, wall[r, :, q].reshape(2 * LANES, w_cols), preferred_element_type=jnp.float32)
+                if q != early[0]:
+                    part = acc[:, columns] + part
+                if q < final:
+                    acc[:, columns] = part
+                else:
+                    o_ref[:, columns] = part.astype(o_ref.dtype)
+
+    def first_products():
+        products(early)
+
     @pl.when(z == 0)
     def _():
         def pushes(p):
@@ -529,6 +555,7 @@
             own = (kvx[p, 0], kvx[p, 1], gates_of(1, p))
             queries_here(p)
             three, two, one = attend_rows([(zin[p, 3], False), (zin[p, 2], False), (qx[p], True)], [lower, own])
+            share(p, 0, 0, 2, *two)
             store_part(p, 1, *three)
             @pl.when(p < direct)
             def _():
@@ -537,7 +564,6 @@
             @pl.when(p >= direct)
             def _():
                 send_part(p, 1, 0, 3)
-            share(p, 0, 0, 2, *two)
             finish(p, one[0])
             share_weights(p)
             passing(p, {0: [near_all, near_lend_all], 2: [on(0)], 4: [on(1)], 7: [on(2)]})
@@ -579,7 +605,7 @@
         each(work)
         def last(p):
             join_two(p)
-            passing(p, {pairs - 2: [lambda: pass_loan(0), near_loan, on(3), lambda: pass_loan(1)]})
+            passing(p, {direct: [lambda: pass_loan(0), near_loan], pairs - 2: [first_products, on(3), lambda: pass_loan(1)]})
         each(last, direct)
 
     @pl.when(z == 3)
@@ -604,12 +630,13 @@
         each(work)
         def last(p):
             join_three(p)
-            passing(p, {3: [on(2)], 4: [lambda: pass_loan(0)], 6: [on(3), lambda: pass_loan(1)]})
+            passing(p, {3: [on(2)], 4: [lambda: pass_loan(0)], 6: [on(3), lambda: pass_loan(1)], 7: [first_products]})
         each(last)
 
     @pl.when(z == 0)
     def _():
         pass_loan(0)
+        first_products()
         pass_on(3)
         pass_loan(1)
 
@@ -617,27 +644,11 @@
     def _():
         pass_loan(0)
         near_loan()
+        first_products()
         pass_on(3)
         pass_loan(1)
 
-    for at, q in enumerate(range(pairs)):
-        landed(wall.at[pl.ds(0, 3), :, q], w_recv.at[q])
-        if at < pairs - 1:
-            o_copy(q).wait_recv()
-        else:
-            @pl.when(z < 2)
-            def _():
-                o_copy(q).wait_recv()
-        lhs = att[q]
-        for r in range(ndp):
-            columns = slice(r * w_cols, (r + 1) * w_cols)
-            part = jnp.dot(lhs, wall[r, :, q].reshape(2 * LANES, w_cols), preferred_element_type=jnp.float32)
-            if at > 0:
-                part = acc[:, columns] + part
-            if at < pairs - 1:
-                acc[:, columns] = part
-            else:
-                o_ref[:, columns] = part.astype(o_ref.dtype)
+    products(late)
 
     g_copy.wait_send()
 

time: 40 us -> 40 us (level)
  no operation moved by 1% of the time
where the time goes in v5:
time: 40 us; the launch traced here: 39.8 us
  Pallas kernels  39 us (98%)
  local copies, waits for them, and re-layouts  0.8 us (2%)
    pallas_call x1, Pallas kernels, fused(): pl.pallas_call(functools.partial(kernel, n, ndp), out_shape=jax.ShapeDtyp...  39 us

profile of v5, /device:TPU:24, one launch (start us, length us, event | category | flops | bytes accessed | tf_op | source)
XLA Modules:
  0.0 39.8 jit_solution(17740332177243099800)
XLA Ops:
  0.0 39.0 %fused_attention.1 = bf16[128,2048]{1,0:T(8,128)(2,1)S(1)} custom-call(bf16[128,2048]{1,0:T(8,128)(2,1)} %bitcast.12, bf16[128,2048]{1,0:T(8,128)(2,1)} %bitcast.13, bf16[128,2048]{1,0:T(8,128)(2,1)} %bitcast.14, f32[2,8,2,128]{3,2,1,0:T(2,128)} %bitcast.15, bf16[2,8,128,512]{3,2,1,0:T(8,128)(2,1)} %bitcast.11), custom_call_target="tpu_custom_call" | custom-call | tf_op jit(solution)/shard_map/fused_attention/pallas_call | solution.py:696
  39.0 0.8 %copy.7 = bf16[1,128,2048]{2,1,0:T(8,128)(2,1)} copy(bf16[1,128,2048]{2,1,0:T(8,128)(2,1)S(1)} %bitcast.10) | data formatting | bytes 1048576

commit v6 on v5

--- a/solution.py
+++ b/solution.py
@@ -237,7 +237,7 @@
     ahead = min(3, pairs)
 
     def lead(makers):
-        for p in range(ahead):
+        for p in range(ahead - (len(makers) > 1)):
             for make in makers:
                 z_own(*make, p).start()
 
@@ -493,15 +493,16 @@
         near_lend(1)
 
     def push(p, makers):
+        reach = ahead - (len(makers) > 1)
         for make in makers:
             z_side(*make, p).start()
-        @pl.when(p + ahead < pairs)
+        @pl.when(p + reach < pairs)
         def _():
             for make in makers:
-                z_own(*make, p + ahead).start()
+                z_own(*make, p + reach).start()
 
     early = [q for q in range(pairs // 2) if q != 1]
-    late = [q for q in range(pairs) if q not in early]
+    late = [q for q in range(pairs - 2) if q not in early] + [pairs - 1, pairs - 2]
 
     def products(which):
         for q in which:
@@ -518,7 +519,7 @@
                 part = jnp.dot(lhs, wall[r, :, q].reshape(2 * LANES, w_cols), preferred_element_type=jnp.float32)
                 if q != early[0]:
                     part = acc[:, columns] + part
-                if q < final:
+                if q != late[-1]:
                     acc[:, columns] = part
                 else:
                     o_ref[:, columns] = part.astype(o_ref.dtype)

time: 40 us -> 40 us (level)
  no operation moved by 1% of the time
where the time goes in v6:
time: 40 us; the launch traced here: 39.8 us
  Pallas kernels  39 us (98%)
  local copies, waits for them, and re-layouts  0.8 us (2%)
    pallas_call x1, Pallas kernels, fused(): pl.pallas_call(functools.partial(kernel, n, ndp), out_shape=jax.ShapeDtyp...  39 us

profile of v6, /device:TPU:24, one launch (start us, length us, event | category | flops | bytes accessed | tf_op | source)
XLA Modules:
  0.0 39.8 jit_solution(3684275970064231324)
XLA Ops:
  0.0 39.0 %fused_attention.1 = bf16[128,2048]{1,0:T(8,128)(2,1)S(1)} custom-call(bf16[128,2048]{1,0:T(8,128)(2,1)} %bitcast.12, bf16[128,2048]{1,0:T(8,128)(2,1)} %bitcast.13, bf16[128,2048]{1,0:T(8,128)(2,1)} %bitcast.14, f32[2,8,2,128]{3,2,1,0:T(2,128)} %bitcast.15, bf16[2,8,128,512]{3,2,1,0:T(8,128)(2,1)} %bitcast.11), custom_call_target="tpu_custom_call" | custom-call | tf_op jit(solution)/shard_map/fused_attention/pallas_call | solution.py:697
  39.0 0.8 %copy.7 = bf16[1,128,2048]{2,1,0:T(8,128)(2,1)} copy(bf16[1,128,2048]{2,1,0:T(8,128)(2,1)S(1)} %bitcast.10) | data formatting | bytes 1048576
